TPU v7x, 32 devices: a whole 2x2x4 slice. The times are simulated.
32 devices in a mesh: sp: 8 (over z, x), tp: 4 (over y, core).
Axes of the slice: x: 2, y: 2, z: 4, core: 2. Of those that a mesh axis runs over, the one named last changes fastest.
Arguments:
- tokens: bfloat16 [2048, 4096], P('sp', 'tp'), may hold values from -6 to 6
- pre_gain: float32 [4096], replicated, may hold values from 0.1 to 1.9
- rate_factor: float32 [2048], P('sp'), may hold values from 0.5 to 2, as said below
- w_rec_in: bfloat16 [4096, 1024], P(None, 'tp'), may hold values from -0.09375 to 0.09375
- w_rec_gate: bfloat16 [4096, 1024], P(None, 'tp')
- conv_taps: float32 [4, 1024], P(None, 'tp'), may hold values from -3 to 3
- rate_maps: bfloat16 [8, 128, 128], P('tp'), may hold values from -0.5 to 0.5
- input_maps: bfloat16 [8, 128, 128], P('tp'), may hold values from -0.5 to 0.5
- decay_param: float32 [1024], P('tp'), as said below
- w_query: bfloat16 [4096, 1536], P(None, 'tp'), may hold values from -0.09375 to 0.09375
- w_latent: bfloat16 [4096, 512], replicated, may hold values from -0.09375 to 0.09375
- w_rope_key: bfloat16 [4096, 64], replicated, may hold values from -0.09375 to 0.09375
- latent_gain: float32 [512], replicated, may hold values from 0.7 to 100, as said below
- w_expand: bfloat16 [512, 2048], P(None, 'tp')
- rec_gain: float32 [1024], P('tp'), may hold values from 0.1 to 1.9
- att_gain: float32 [1024], P('tp'), may hold values from 0.1 to 1.9
- w_out_rec: bfloat16 [1024, 4096], P('tp'), may hold values from -0.125 to 0.125
- w_out_att: bfloat16 [1024, 4096], P('tp'), may hold values from -0.125 to 0.125
- post_gain: float32 [4096], replicated, may hold values from 0.1 to 1.9
Outputs:
- layer_out: bfloat16 [2048, 4096], P(('sp', 'tp'))
Inputs may be any that keep to these rules, and one draw needn't show every extreme that they name: `rate_factor`: one positive factor for each position. `decay_param`: one parameter for each recurrent channel. `latent_gain`: one positive gain for each latent entry.
All inputs are finite; a program needn't handle non-finite values.
Results may differ from a plain program's by a relative error of at most 0.017.
The roundings to bfloat16 on the way count: a program that leaves them out, or rounds other values in their place, can miss the bound.
Values may be sent and summed in bfloat16 or wider, within the bound.
A program may use at most 128 MiB of HBM per device.

v0:
```python
import functools
import math

import jax
import jax.numpy as jnp
from jax import lax
from jax.experimental import pallas as pl
from jax.experimental.pallas import tpu as pltpu
from jax.sharding import PartitionSpec as P

NOPE = 128
ROPE = 64
VDIM = 128


EPS = 1e-06
RATE_C = 8.0
THETA = 10000.0
span_limit = 2048


def passed_along(block, axis, distance):
    devices = range(lax.axis_size(axis))
    route = [(i - distance, i) for i in devices if i - distance in devices]
    return lax.ppermute(block, axis, route)


def entering(value, axis, join, neutral):
    count, mine = (lax.axis_size(axis), lax.axis_index(axis))
    pieces = jax.tree.map(lambda part: lax.all_gather(part, axis), value)
    subtotal = jax.tree.map(
        lambda part, zero: jnp.full_like(part, 0) + jnp.asarray(zero, part.dtype), value, neutral
    )

    def step(position, subtotal):
        longer = join(subtotal, jax.tree.map(lambda part: part[position], pieces))
        return jax.tree.map(lambda new, old: jnp.where(position < mine, new, old), longer, subtotal)

    return lax.fori_loop(0, count - 1, step, subtotal)


def rms_inverse(values):
    return lax.rsqrt(jnp.mean(values * values, axis=-1, keepdims=True) + EPS)


def rotate(values, cosine, sine_part):
    half_width = values.shape[-1] // 2
    leading = values[..., :half_width]
    trailing = values[..., half_width:]
    return jnp.concatenate(
        [leading * cosine - trailing * sine_part, trailing * cosine + leading * sine_part], axis=-1
    )


def angles(length, offset, span_width):
    frequency = 1.0 / THETA ** (jnp.arange(0, span_width, 2).astype(jnp.float32) / span_width)
    places = (offset + jnp.arange(length)).astype(jnp.float32)
    turned = places[:, None] * frequency[None, :]
    return (jnp.cos(turned), jnp.sin(turned))


def combine_steps(earlier, later):
    return (earlier[0] * later[0], later[0] * earlier[1] + later[1])


def attend_block(state_now, query_nope, query_rope, places, keys_nope, key_rope, values, key_root):
    maxima, totals, accumulated = state_now
    scaling = 1.0 / math.sqrt(query_nope.shape[-1] + query_rope.shape[-1])
    scores = jnp.einsum("qhd,khd->hqk", query_nope, keys_nope, preferred_element_type=jnp.float32)
    scores = scores + jnp.einsum(
        "qhd,kd->hqk", query_rope, key_rope, preferred_element_type=jnp.float32
    )
    scores = scores * scaling
    key_places = key_root + jnp.arange(keys_nope.shape[0])
    visible = key_places[None, :] <= places[:, None]
    scores = jnp.where(visible[None], scores, -jnp.inf)
    largest = jnp.maximum(maxima, jnp.max(scores, axis=-1))
    anchor = jnp.where(largest == -jnp.inf, 0.0, largest)
    weights = jnp.exp(scores - anchor[..., None])
    shrink = jnp.exp(maxima - anchor)
    totals = totals * shrink + jnp.sum(weights, axis=-1)
    accumulated = accumulated * shrink[..., None] + jnp.einsum(
        "hqk,khd->hqd", weights.astype(jnp.bfloat16), values, preferred_element_type=jnp.float32
    )
    return (largest, totals, accumulated)


MESH = pl.DeviceIdType.MESH


def one_minus_exp(y):
    series = 1.0 + y * (1.0 / 8.0)
    for order in (7, 6, 5, 4, 3, 2):
        series = 1.0 + y * (1.0 / order) * series
    return jnp.where(y > -0.5, -y * series, 1.0 - jnp.exp(y))


def gelu_tanh(x):
    inner = math.sqrt(2.0 / math.pi) * (x + 0.044715 * (x * x * x))
    return 0.5 * x * (1.0 + jnp.tanh(inner))


def rec_kernel(
    n, rec_ref, taps_ref, rmap_ref, imap_ref, soft_ref, rate_ref, gate_ref,
    out_ref, sq_ref, padded, tail_tx, tail_rx, carry_tx, carry_rx, sems, rsems,
):
    me = lax.axis_index("sp")
    rows, channels = rec_ref.shape
    barrier = pltpu.get_barrier_semaphore()
    for d in range(1, n):
        pl.semaphore_signal(
            barrier, inc=1, device_id={"sp": lax.rem(me + d, n)}, device_id_type=MESH
        )
    x = rec_ref[...].astype(jnp.float32)
    tail_tx[...] = x[rows - 8 :, :]
    padded[8:, :] = x
    pl.semaphore_wait(barrier, n - 1)
    tail = pltpu.make_async_remote_copy(
        src_ref=tail_tx, dst_ref=tail_rx, send_sem=sems.at[0], recv_sem=rsems.at[0],
        device_id={"sp": lax.rem(me + 1, n)}, device_id_type=MESH,
    )
    tail.start()
    tail.wait()
    padded[0:8, :] = jnp.where(me > 0, tail_rx[...], 0.0)
    count = taps_ref.shape[0]
    conv = taps_ref[0:1, :] * padded[9 - count : 9 - count + rows, :]
    for k in range(1, count):
        conv = conv + taps_ref[k : k + 1, :] * padded[9 - count + k : 9 - count + k + rows, :]
    low = conv.astype(jnp.bfloat16)
    width = rmap_ref.shape[1]
    rate, entry = [], []
    for b in range(rmap_ref.shape[0]):
        part = low[:, b * width : (b + 1) * width]
        rate.append(jnp.dot(part, rmap_ref[b], preferred_element_type=jnp.float32))
        entry.append(jnp.dot(part, imap_ref[b], preferred_element_type=jnp.float32))
    rate = jax.nn.sigmoid(jnp.concatenate(rate, axis=1))
    entry = jax.nn.sigmoid(jnp.concatenate(entry, axis=1))
    log_keep = -RATE_C * rate_ref[...] * rate * soft_ref[...]
    a = jnp.exp(log_keep)
    b = jnp.sqrt(one_minus_exp(2.0 * log_keep)) * entry * conv
    row = lax.broadcasted_iota(jnp.int32, (rows, channels), 0)
    d = 1
    while d < rows:
        inside = row >= d
        b = a * jnp.where(inside, pltpu.roll(b, d, 0), 0.0) + b
        a = a * jnp.where(inside, pltpu.roll(a, d, 0), 1.0)
        d *= 2
    carry_tx[...] = jnp.zeros_like(carry_tx)
    carry_tx[0:1, :] = a[rows - 1 :, :]
    carry_tx[1:2, :] = b[rows - 1 :, :]
    copies = []
    for d in range(1, n):
        copies.append(
            pltpu.make_async_remote_copy(
                src_ref=carry_tx, dst_ref=carry_rx.at[me], send_sem=sems.at[d],
                recv_sem=rsems.at[d], device_id={"sp": lax.rem(me + d, n)}, device_id_type=MESH,
            )
        )
        copies[-1].start()
    gated = gelu_tanh(gate_ref[...])
    for copy in copies:
        copy.wait()
    carried = jnp.zeros((1, channels), jnp.float32)
    for s in range(n - 1):
        longer = carry_rx[s, 0:1, :] * carried + carry_rx[s, 1:2, :]
        carried = jnp.where(s < me, longer, carried)
    rec_out = (b + a * carried) * gated
    out_ref[...] = rec_out
    sq_ref[...] = jnp.sum(rec_out * rec_out, axis=1, keepdims=True)


def recurrent(rec_input, conv_taps, rate_maps, input_maps, soft, rate, gate_value):
    n = lax.axis_size("sp")
    rows, channels = rec_input.shape
    vmem = pl.BlockSpec(memory_space=pltpu.VMEM)
    return pl.pallas_call(
        functools.partial(rec_kernel, n),
        out_shape=(
            jax.ShapeDtypeStruct((rows, channels), jnp.float32),
            jax.ShapeDtypeStruct((rows, 1), jnp.float32),
        ),
        in_specs=[vmem] * 7,
        out_specs=(vmem, vmem),
        scratch_shapes=[
            pltpu.VMEM((rows + 8, channels), jnp.float32),
            pltpu.VMEM((8, channels), jnp.float32),
            pltpu.VMEM((8, channels), jnp.float32),
            pltpu.VMEM((8, channels), jnp.float32),
            pltpu.VMEM((n, 8, channels), jnp.float32),
            pltpu.SemaphoreType.DMA((n,)),
            pltpu.SemaphoreType.DMA((n,)),
        ],
        compiler_params=pltpu.CompilerParams(collective_id=0, has_side_effects=True),
        cost_estimate=pl.CostEstimate(flops=20_000_000, bytes_accessed=2_000_000, transcendentals=0),
        name="recurrent",
    )(rec_input, conv_taps, rate_maps, input_maps, soft, rate, gate_value)


def shards(
    tokens,
    pre_gain,
    rate_factor,
    w_rec_in,
    w_rec_gate,
    conv_taps,
    rate_maps,
    input_maps,
    decay_param,
    w_query,
    w_latent,
    w_rope_key,
    latent_gain,
    w_expand,
    rec_gain,
    att_gain,
    w_out_rec,
    w_out_att,
    post_gain,
):
    row_count = tokens.shape[0]
    model_width = w_rec_in.shape[0]
    channels = w_rec_in.shape[1]
    heads_here = w_query.shape[1] // (NOPE + ROPE)
    group_size = lax.axis_size("tp")
    first_place = lax.axis_index("sp") * row_count
    places = first_place + jnp.arange(row_count)
    last_place = first_place + row_count - 1
    piece_wide = lax.all_gather(tokens, "tp", axis=1, tiled=True).astype(jnp.float32)
    piece_low = (piece_wide * pre_gain).astype(jnp.bfloat16)

    def accumulate(source, weight):
        return jnp.dot(source, weight, preferred_element_type=jnp.float32)

    squares = jnp.sum(piece_wide * piece_wide, axis=1, keepdims=True)
    sum_input = accumulate(piece_low, w_rec_in)
    sum_gate = accumulate(piece_low, w_rec_gate)
    sum_query = accumulate(piece_low, w_query)
    sum_latent = accumulate(piece_low, w_latent)
    sum_rope = accumulate(piece_low, w_rope_key)
    inverse = lax.rsqrt(squares / model_width + EPS)
    rec_input = (inverse * sum_input).astype(jnp.bfloat16)
    gate_value = inverse * sum_gate
    query_raw = inverse * sum_query
    latent_raw = inverse * sum_latent
    rope_raw = inverse * sum_rope
    rec_out, rec_squares = recurrent(
        rec_input,
        conv_taps,
        rate_maps,
        input_maps,
        jax.nn.softplus(-decay_param)[None, :],
        rate_factor[:, None],
        gate_value,
    )
    cosine, sine_part = angles(row_count, first_place, ROPE)
    query_heads = query_raw.reshape(row_count, heads_here, NOPE + ROPE)
    query_nope = query_heads[:, :, :NOPE].astype(jnp.bfloat16)
    query_rope = rotate(query_heads[:, :, NOPE:], cosine[:, None, :], sine_part[:, None, :]).astype(
        jnp.bfloat16
    )
    own_latent = (latent_raw * rms_inverse(latent_raw) * latent_gain).astype(jnp.bfloat16)
    rope_key = rotate(rope_raw, cosine, sine_part).astype(jnp.bfloat16)
    start_state = (
        jnp.full((heads_here, row_count), -jnp.inf, jnp.float32),
        jnp.zeros((heads_here, row_count), jnp.float32),
        jnp.zeros((heads_here, row_count, VDIM), jnp.float32),
    )
    expanded_local = jnp.dot(own_latent, w_expand, preferred_element_type=jnp.float32).astype(
        jnp.bfloat16
    )
    key_source = lax.all_gather(expanded_local, "sp", axis=0, tiled=True)
    rope_source = lax.all_gather(rope_key, "sp", axis=0, tiled=True)
    total_rows = key_source.shape[0]
    key_span = math.gcd(total_rows, span_limit)

    def one_span(span_index, state_inner):
        key_root = span_index * key_span

        def compute(state_deep):
            source_rows = lax.dynamic_slice_in_dim(key_source, span_index * key_span, key_span, 0)
            rope_rows = lax.dynamic_slice_in_dim(rope_source, span_index * key_span, key_span, 0)
            expanded = source_rows
            expanded = expanded.reshape(key_span, heads_here, NOPE + VDIM)
            return attend_block(
                state_deep,
                query_nope,
                query_rope,
                places,
                expanded[:, :, :NOPE],
                rope_rows,
                expanded[:, :, NOPE:],
                key_root,
            )

        def keep_state(state_deep):
            return state_deep

        return lax.cond(key_root <= last_place, compute, keep_state, state_inner)

    maxima, totals, accumulated = lax.fori_loop(0, total_rows // key_span, one_span, start_state)
    att_out = (
        (accumulated / totals[..., None]).transpose(1, 0, 2).reshape(row_count, heads_here * VDIM)
    )
    att_squares = jnp.sum(att_out * att_out, axis=1, keepdims=True)
    rec_total, att_total = lax.psum((rec_squares, att_squares), "tp")
    rec_norm = (rec_out * lax.rsqrt(rec_total / (channels * group_size) + EPS) * rec_gain).astype(
        jnp.bfloat16
    )
    att_norm = (
        att_out * lax.rsqrt(att_total / (heads_here * VDIM * group_size) + EPS) * att_gain
    ).astype(jnp.bfloat16)
    mixed_sum = lax.psum_scatter(
        (
            jnp.dot(rec_norm, w_out_rec, preferred_element_type=jnp.float32)
            + jnp.dot(att_norm, w_out_att, preferred_element_type=jnp.float32)
        ).astype(jnp.bfloat16),
        "tp",
        scatter_dimension=0,
        tiled=True,
    ).astype(jnp.float32)
    return (mixed_sum * rms_inverse(mixed_sum) * post_gain).astype(jnp.bfloat16)


def solution(mesh):
    placed = (
        P("sp", "tp"),
        P(),
        P("sp"),
        P(None, "tp"),
        P(None, "tp"),
        P(None, "tp"),
        P("tp", None, None),
        P("tp", None, None),
        P("tp"),
        P(None, "tp"),
        P(),
        P(),
        P(),
        P(None, "tp"),
        P("tp"),
        P("tp"),
        P("tp", None),
        P("tp", None),
        P(),
    )
    return jax.shard_map(
        shards, mesh=mesh, in_specs=placed, out_specs=P(("sp", "tp"), None), check_vma=False
    )
```

profile of v0, /device:TPU:24, one launch (start us, length us, event | category | flops | bytes accessed | tf_op | source)
XLA Modules:
  0.0 178.2 jit_solution(3048201556429894492)
XLA Ops:
  6.5 0.0 all-gather.3.cloned.1.call-start
  6.5 0.7 all-gather.3.cloned.1.call-update
  7.3 0.0 all-gather.5.cloned.1.call-start
  7.3 25.2 %all-gather.3.cloned.1.call-done = bf16[256,4096]{1,0:T(8,128)(2,1)} async-done(((bf16[256,1024]{1,0:T(8,128)(2,1)}), bf16[256,4096]{1,0:T(8,128)(2,1)}) %all-gather.3.cloned.1.call-update) | async-done | bytes 2097168 | tf_op jit(solution)/shard_map/all_gather | solution.py:228
  32.5 2.2 %fusion.15 = f32[256]{0:T(256)S(1)} fusion(bf16[256,4096]{1,0:T(8,128)(2,1)} %all-gather.3.cloned.1.call-done), kind=kLoop, calls=%fused_computation.23 | loop fusion | flops 3145472 | bytes 2098176 | tf_op jit(solution)/shard_map/reduce_sum | solution.py:234
  34.7 0.0 copy-start.6
  34.7 0.0 copy-start.9
  34.8 0.0 copy-start.10
  34.8 0.0 copy-start.12
  34.8 3.6 %multiply_reduce_fusion = (f32[256]{0:T(256)S(1)}, f32[256,512]{1,0:T(8,128)S(1)}) fusion(bf16[4096,512]{1,0:T(8,128)(2,1)} %param.31, bf16[256,4096]{1,0:T(8,128)(2,1)S(1)} %copy-done.2, f32[4096]{0:T(1024)S(1)} %copy-done.14, f32[256]{0:T(256)S(1)} %add_rsqrt_fusion.1), kind=kOutput, calls=%fused_computation.38 | convolution fusion | flops 1077280512 | bytes 6834176 | tf_op jit(solution)/shard_map/dot_general | solution.py:232
  38.4 0.0 copy-done.6
  38.4 0.0 copy-done.9
  38.4 1.1 convolution_convert_fusion
  39.4 0.0 all-gather.5.cloned.1.call-update
  39.5 0.0 reduce-scatter.2.cloned.1.call-start
  39.5 0.8 copy.27.rate_ref
  40.4 0.6 compare_select_fusion.1
  41.0 3.6 %convolution_multiply_fusion.1 = f32[256,384]{1,0:T(8,128)} fusion(bf16[4096,384]{1,0:T(8,128)(2,1)S(1)} %copy-done, bf16[256,4096]{1,0:T(8,128)(2,1)} %all-gather.3.cloned.1.call-done, f32[4096]{0:T(1024)S(1)} %copy-done.14, f32[256]{0:T(256)S(1)} %add_rsqrt_fusion.1), kind=kOutput, calls=%fused_computation.29 | convolution fusion | flops 808550400 | bytes 5653504 | tf_op jit(solution)/shard_map/dot_general | solution.py:232
  44.6 1.9 %copy.28 = f32[256,384]{0,1:T(8,128)} copy(f32[256,384]{1,0:T(8,128)} %convolution_multiply_fusion.1) | data formatting | bytes 786432 | tf_op jit(solution)/shard_map/mul | solution.py:243
  46.5 3.9 %convolution_multiply_fusion.2.gate_ref = f32[256,256]{1,0:T(8,128)} fusion(bf16[4096,256]{1,0:T(8,128)(2,1)} %param.25, bf16[256,4096]{1,0:T(8,128)(2,1)} %all-gather.3.cloned.1.call-done, f32[4096]{0:T(1024)S(1)} %copy-done.14, f32[256]{0:T(256)S(1)} %add_rsqrt_fusion.1), kind=kOutput, calls=%fused_computation.30 | convolution fusion | flops 540082176 | bytes 4473856 | tf_op jit(solution)/shard_map/dot_general | solution.py:232
  50.4 1.4 fusion.17.rec_ref
  51.8 12.9 %recurrent.1 = (f32[256,256]{1,0:T(8,128)}, f32[256,1]{1,0:T(8,128)}) custom-call(bf16[256,256]{1,0:T(8,128)(2,1)} %fusion.17.rec_ref, f32[4,256]{1,0:T(4,128)} %taps_ref.1, bf16[2,128,128]{2,1,0:T(8,128)(2,1)} %rmap_ref.1, bf16[2,128,128]{2,1,0:T(8,128)(2,1)} %imap_ref.1, f32[1,256]{1,0:T(1,128)} %bitcast.42, f32[256,1]{1,0:T(8,128)} %copy.27.rate_ref, ...), custom_call_target="tpu_custom_call" | custom-call | flops 20000000 | bytes 2000000 | tf_op jit(solution)/shard_map/recurrent/pallas_call | solution.py:176
  64.7 2.4 %convolution_multiply_fusion.4 = f32[256,64]{0,1:T(8,128)S(1)} fusion(bf16[4096,64]{0,1:T(8,128)(2,1)} %param.32, bf16[256,4096]{1,0:T(8,128)(2,1)} %all-gather.3.cloned.1.call-done, f32[4096]{0:T(1024)S(1)} %copy-done.14, f32[256]{0:T(256)S(1)} %add_rsqrt_fusion.1), kind=kOutput, calls=%fused_computation.33 | convolution fusion | flops 137379840 | bytes 2704384 | tf_op jit(solution)/shard_map/dot_general | solution.py:232
  67.2 0.2 multiply_cosine_fusion
  67.4 0.9 subtract_convert_fusion
  68.3 30.9 %all_gather.11 = bf16[2048,64]{0,1:T(8,128)(2,1)} all-gather(bf16[256,64]{0,1:T(8,128)(2,1)S(1)} %pad_maximum_fusion.1), channel_id=1, replica_groups=mesh['sp'=8,'tp'=4] {'sp'}, dimensions={0}, use_global_device_ids=true | all-gather | bytes 294912 | tf_op jit(solution)/shard_map/all_gather | solution.py:272
  99.3 14.6 %conditional.1 = (f32[2,256]{1,0:T(2,128)S(1)}, f32[2,256,128]{1,2,0:T(8,128)}) conditional(s32[]{:T(128)} %convert_element_type.61, (f32[2,256]{1,0:T(2,128)S(1)}, f32[2,256,128]{2,1,0:T(8,128)S(1)}) %tuple.25, (s32[]{:T(128)}, s32[256]{0:T(256)S(1)}, bf16[2048,512]{1,0:T(8,128)(2,1)}, f32[256,2,192]{0,2,1:T(8,128)}, bf16[2048,64]{0,1:T(8,128)(2,1)}, ...), branch_computations={%region_3.0_spmd, %region_4.7_spmd} | conditional | flops 680135424 | bytes 39873612 | solution.py:298
  99.3 4.0 %copy.29 = bf16[2048,512]{0,1:T(8,128)(2,1)} copy(bf16[2048,512]{1,0:T(8,128)(2,1)} %get-tuple-element.148) | data formatting | bytes 4194304 | tf_op jit(solution)/shard_map
  103.3 1.8 %copy.30 = bf16[256,2,192]{2,0,1:T(8,128)(2,1)} copy(f32[256,2,192]{0,2,1:T(8,128)} %get-tuple-element.149) | data formatting | bytes 589824 | tf_op jit(solution)/shard_map
  105.1 2.0 %fusion.11 = f32[2,256,2048]{2,1,0:T(8,128)S(1)} fusion(bf16[2048,2,256]{0,2,1:T(8,128)(2,1)} %bitcast.37, bf16[256,2,192]{2,0,1:T(8,128)(2,1)} %copy.30), kind=kOutput, calls=%fused_computation.11 | convolution fusion | flops 268435456 | bytes 5373952 | tf_op jit(solution)/shard_map/while/body/eval_jaxpr/cond/branch_1_fun/qhd,khd->hqk/dot_general | solution.py:69
  107.1 0.4 iota_compare_fusion
  107.5 1.3 fusion.34
  108.9 0.7 fusion.3
  109.6 0.9 copy-done.1
  110.5 1.6 fusion.7
  112.0 1.8 %copy.35 = f32[2,256,128]{1,2,0:T(8,128)} copy(f32[2,256,128]{2,1,0:T(8,128)} %fusion.7) | data formatting | bytes 524288 | tf_op jit(solution)/shard_map/while/body/eval_jaxpr/cond | solution.py:298
  113.8 1.0 fusion.28
  114.8 0.1 copy.32
  115.0 13.3 %all-reduce = (f32[256,1]{1,0:T(8,128)}, f32[256,1]{1,0:T(8,128)}) all-reduce(f32[256,1]{1,0:T(8,128)} %get-tuple-element.133, f32[256,1]{1,0:T(8,128)S(1)} %copy.32), channel_id=1, replica_groups=mesh['sp'=8,'tp'=4] {'tp'}, use_global_device_ids=true, to_apply=%region_1.2 | all-reduce | flops 512 | bytes 4096 | tf_op jit(solution)/shard_map/psum | solution.py:305
  128.3 1.1 rsqrt_reduce_fusion
  129.4 0.1 fusion.27
  129.5 0.0 copy-start.4
  129.5 2.6 %fusion.31 = f32[256,4096]{1,0:T(8,128)S(1)} fusion(bf16[256,4096]{1,0:T(8,128)(2,1)} %param.37, f32[256,256]{1,0:T(8,128)} %get-tuple-element.132, f32[256]{0:T(256)S(1)} %copy-done.8, f32[256]{0:T(256)S(1)} %get-tuple-element.176), kind=kOutput, calls=%fused_computation.47 | convolution fusion | flops 537067520 | bytes 6555648 | tf_op jit(solution)/shard_map/dot_general | solution.py:314
  132.1 2.1 %fusion.14 = bf16[256,4096]{1,0:T(8,128)(2,1)} fusion(f32[256,4096]{1,0:T(8,128)S(1)} %fusion.31, bf16[256,256]{0,1:T(8,128)(2,1)S(1)} %fusion.27, bf16[256,4096]{1,0:T(8,128)(2,1)S(1)} %copy-done.4), kind=kOutput, calls=%fused_computation.22 | convolution fusion | flops 538968064 | bytes 8519680 | tf_op jit(solution)/shard_map/dot_general | solution.py:315
  134.2 0.0 reduce-scatter.2.cloned.1.call-update
  134.2 34.2 %reduce-scatter.2.cloned.1.call-done = bf16[64,4096]{1,0:T(8,128)(2,1)} async-done(((bf16[256,4096]{1,0:T(8,128)(2,1)}), bf16[64,4096]{1,0:T(8,128)(2,1)}) %reduce-scatter.2.cloned.1.call-update) | async-done | bytes 524304 | tf_op jit(solution)/shard_map/reduce_scatter | solution.py:312
  168.4 1.2 fusion.23
  169.7 2.0 %fusion.25 = bf16[64,4096]{1,0:T(8,128)(2,1)} fusion(bf16[64,4096]{1,0:T(8,128)(2,1)} %reduce-scatter.2.cloned.1.call-done, f32[4096]{0:T(1024)S(1)} %copy-done.7, f32[64]{0:T(128)S(1)} %add_rsqrt_fusion.2), kind=kLoop, calls=%fused_computation.36 | loop fusion | flops 1048576 | bytes 1065216 | tf_op jit(solution)/shard_map/convert_element_type | solution.py:321
  (36 shorter events, 0.1 us)
Async XLA Ops:
  6.5 34.4 %copy-start = (bf16[4096,384]{1,0:T(8,128)(2,1)S(1)}, bf16[4096,384]{1,0:T(8,128)(2,1)}, u32[]{:S(2)}) copy-start(bf16[4096,384]{1,0:T(8,128)(2,1)} %param.30) | copy-start | bytes 9437188
  6.5 28.2 %copy-start.14 = (f32[4096]{0:T(1024)S(1)}, f32[4096]{0:T(1024)}, u32[]{:S(2)}) copy-start(f32[4096]{0:T(1024)} %param.22) | copy-start | bytes 49156
  6.5 25.9 %all-gather.3.cloned.1.call-start = ((), (), s32[]{:S(2)}) async-start(), calls=%async_computation.1 | async-start | bytes 2621440 | tf_op jit(solution)/shard_map/all_gather | solution.py:228
  7.3 92.0 %all-gather.5.cloned.1.call-start = ((), (), s32[]{:S(2)}) async-start(), calls=%async_computation.2 | async-start | bytes 2359296 | tf_op jit(solution)/shard_map/all_gather | solution.py:271
  32.5 2.3 %copy-start.2 = (bf16[256,4096]{1,0:T(8,128)(2,1)S(1)}, bf16[256,4096]{1,0:T(8,128)(2,1)}, u32[]{:S(2)}) copy-start(bf16[256,4096]{1,0:T(8,128)(2,1)} %all-gather.3.cloned.1.call-done) | copy-start | bytes 6291460
  34.7 3.6 %copy-start.6 = (bf16[512,512]{1,0:T(8,128)(2,1)S(1)}, bf16[512,512]{1,0:T(8,128)(2,1)}, u32[]{:S(2)}) copy-start(bf16[512,512]{1,0:T(8,128)(2,1)} %param.34) | copy-start | bytes 1572868
  34.7 3.6 %copy-start.9 = (f32[512]{0:T(512)S(1)}, f32[512]{0:T(512)}, u32[]{:S(2)}) copy-start(f32[512]{0:T(512)} %param.33) | copy-start | bytes 6148
  34.8 4.8 %copy-start.10 = (f32[256]{0:T(256)S(1)}, f32[256]{0:T(256)}, u32[]{:S(2)}) copy-start(f32[256]{0:T(256)} %param.23) | copy-start | bytes 3076
  34.8 5.6 %copy-start.12 = (f32[256]{0:T(256)S(1)}, f32[256]{0:T(256)}, u32[]{:S(2)}) copy-start(f32[256]{0:T(256)} %param.29) | copy-start | bytes 3076
  39.5 128.9 %reduce-scatter.2.cloned.1.call-start = ((), (), s32[]{:S(2)}) async-start(), calls=%async_computation.3 | async-start | bytes 2621440 | tf_op jit(solution)/shard_map/reduce_scatter | solution.py:312
  46.5 3.9 %copy-start.3 = (bf16[256,4096]{1,0:T(8,128)(2,1)S(1)}, bf16[256,4096]{1,0:T(8,128)(2,1)}, u32[]{:S(2)}) copy-start(bf16[256,4096]{1,0:T(8,128)(2,1)} %all-gather.3.cloned.1.call-done) | copy-start | bytes 6291460
  46.5 3.9 %copy-start.13 = (bf16[4096,256]{1,0:T(8,128)(2,1)S(1)}, bf16[4096,256]{1,0:T(8,128)(2,1)}, u32[]{:S(2)}) copy-start(bf16[4096,256]{1,0:T(8,128)(2,1)} %param.24) | copy-start | bytes 6291460
  99.3 30.1 %copy-start.11 = (f32[256]{0:T(256)S(1)}, f32[256]{0:T(256)}, u32[]{:S(2)}) copy-start(f32[256]{0:T(256)} %param.36) | copy-start | bytes 3076
  99.3 30.2 %copy-start.8 = (f32[256]{0:T(256)S(1)}, f32[256]{0:T(256)}, u32[]{:S(2)}) copy-start(f32[256]{0:T(256)} %param.35) | copy-start | bytes 3076
  105.1 2.4 %copy-start.5 = (bf16[2048,64]{0,1:T(8,128)(2,1)S(1)}, bf16[2048,64]{0,1:T(8,128)(2,1)}, u32[]{:S(2)}) copy-start(bf16[2048,64]{0,1:T(8,128)(2,1)} %get-tuple-element.125) | copy-start | bytes 786436 | tf_op jit(solution)/shard_map/while/body/eval_jaxpr/cond
  108.9 1.6 copy-start.1
  129.5 2.6 %copy-start.4 = (bf16[256,4096]{1,0:T(8,128)(2,1)S(1)}, bf16[256,4096]{1,0:T(8,128)(2,1)}, u32[]{:S(2)}) copy-start(bf16[256,4096]{1,0:T(8,128)(2,1)} %param.38) | copy-start | bytes 6291460
  134.2 35.5 %copy-start.7 = (f32[4096]{0:T(1024)S(1)}, f32[4096]{0:T(1024)}, u32[]{:S(2)}) copy-start(f32[4096]{0:T(1024)} %param.39) | copy-start | bytes 49156
Sparse Core Ops, SparseCore 0:
  8.9 23.5 all-gather.2
  39.6 50.8 all-gather.4
  134.3 34.0 reduce-scatter.1
where the time goes:
time: 181 us; the launch traced here: 178 us
  waiting for transfers between devices  60.1 us (33%)
  blocking collectives  44.2 us (24%)
  matrix products  25.6 us (14%)
  between operations  13.3 us (7%)
  Pallas kernels  12.9 us (7%)
  local copies, waits for them, and re-layouts  11.4 us (6%)
  other arithmetic  10.6 us (6%)
    reduce_scatter x1, waiting for transfers between devices, shards(): lax.psum_scatter((jnp.dot(rec_norm, w_out_rec, preferred_element_type=jnp...  34.2 us
    all_gather x1, blocking collectives, shards(): rope_source = lax.all_gather(rope_key, 'sp', axis=0, tiled=True)  30.9 us
    all_gather x1, waiting for transfers between devices, shards(): lax.all_gather(tokens, 'tp', axis=1, tiled=True).astype(jnp.float32)  25.2 us
    dot_general x5, matrix products, accumulate(): return jnp.dot(source, weight, preferred_element_type=jnp.float32)  14.9 us
    psum x1, blocking collectives, shards(): rec_total, att_total = lax.psum((rec_squares, att_squares), 'tp')  13.3 us
    pallas_call x1, Pallas kernels, recurrent(): pl.pallas_call(functools.partial(rec_kernel, n), out_shape=(jax.ShapeDtyp...  12.9 us
    another operation x2, local copies, waits for them, and re-layouts  5.8 us
  transfers between devices with their start and end apart: 3, of which 2 were waited for; matrix products, arithmetic and copies ran while one was open for 9% of the time, Pallas kernels for 7%

commit v1 on v0

v1 whole, which is shorter than its diff:
```python
import functools
import math

import jax
import jax.numpy as jnp
from jax import lax
from jax.experimental import pallas as pl
from jax.experimental.pallas import tpu as pltpu
from jax.sharding import PartitionSpec as P

NOPE = 128
ROPE = 64
VDIM = 128
LANES = 128

EPS = 1e-06
RATE_C = 8.0
THETA = 10000.0
CHUNKS = 4
COLS = 4

MESH = pl.DeviceIdType.MESH
F32 = jnp.float32
BF16 = jnp.bfloat16


def one_minus_exp(y):
    series = 1.0 + y * (1.0 / 8.0)
    for order in (7, 6, 5, 4, 3, 2):
        series = 1.0 + y * (1.0 / order) * series
    return jnp.where(y > -0.5, -y * series, 1.0 - jnp.exp(y))


def gelu_tanh(x):
    inner = math.sqrt(2.0 / math.pi) * (x + 0.044715 * (x * x * x))
    return 0.5 * x * (1.0 + jnp.tanh(inner))


def softplus(x):
    z = jnp.exp(-jnp.abs(x))
    w = z / (2.0 + z)
    w2 = w * w
    series = jnp.full_like(w, 1.0 / 17.0)
    for order in (15, 13, 11, 9, 7, 5, 3):
        series = 1.0 / order + w2 * series
    return jnp.maximum(x, 0.0) + 2.0 * (w + w * w2 * series)


def rotate(tile, cosine, sine):
    lane = lax.broadcasted_iota(jnp.int32, tile.shape, 1)
    half = ROPE // 2
    other = jnp.where(
        lane < half, pltpu.roll(tile, tile.shape[1] - half, 1), pltpu.roll(tile, half, 1)
    )
    return tile * cosine + other * sine


def fused_kernel(
    n_sp, n_tp, heads,
    tokens, pre_gain, rate_factor, w_rec, w_gate, taps_in, rmap_in, imap_in, decay_in, w_query,
    w_latent, w_rope, lat_gain_in, w_expand, rec_gain_in, att_gain_in, w_or, w_oa, post_gain_in,
    cos_in, sin_in,
    out_ref,
    tok, scaled, gain, rate, wrec, wgate, taps, rmap, imap, decay, wq, wlat, wrope, lgain, wexp,
    rgain, again, wor, woa, pgain, cosv, sinv,
    acc_lat, acc_rope, acc_rec, acc_gate, acc_q, sq, kv, qcat, padded, gated,
    m_ref, l_ref, o_ref, a_ref, b_ref, rb, ab,
    tail_tx, tail_rx, carry_tx, carry_rx, sq_tx, sq_rx, inv_r, inv_a,
    pr, comb, d2d_tx, d2d_rx, y_tx, y_rx, mixed,
    load_sem, own_tx, own_rx, tok_tx, tok_rx, fwd_tx, fwd_rx,
    kvz_tx, kvx_tx, kv_rx, kvd_tx, kvd_rx,
    tail_s, carry_s, carry_r, sq_s, sq_r, d2d_s, d2d_r, y_s, y_r,
):
    me = lax.axis_index("sp")
    tp = lax.axis_index("tp")
    n_y = n_tp // 2
    levels = n_sp // 2
    core = lax.rem(tp, 2)
    yy = lax.div(tp, 2)
    partner = tp + 1 - 2 * core
    column = lax.rem(me, 2)
    level = lax.div(me, 2)
    neighbour = me + 1 - 2 * column
    rows, feats = tokens.shape
    width = feats * n_tp
    latent = w_latent.shape[1]
    channels = w_rec.shape[1]
    rc = rows // CHUNKS
    hc = rc // 2
    rd = rows // n_tp
    cb = width // COLS

    pairs = (
        (tokens, tok.at[tp]), (pre_gain, gain), (w_latent, wlat), (w_rope, wrope), (w_rec, wrec),
        (w_gate, wgate), (w_query, wq), (lat_gain_in, lgain), (cos_in, cosv), (sin_in, sinv),
        (rate_factor, rate), (taps_in, taps), (rmap_in, rmap), (imap_in, imap), (decay_in, decay),
        (rec_gain_in, rgain), (att_gain_in, again), (w_expand, wexp), (w_or, wor), (w_oa, woa),
        (post_gain_in, pgain),
    )
    loads = [pltpu.make_async_copy(s, d, load_sem.at[i]) for i, (s, d) in enumerate(pairs)]
    for copy in loads:
        copy.start()

    barrier = pltpu.get_barrier_semaphore()
    for d in range(1, n_sp):
        pl.semaphore_signal(
            barrier, inc=1, device_id={"sp": lax.rem(me + d, n_sp)}, device_id_type=MESH
        )
    for d in range(1, n_tp):
        pl.semaphore_signal(
            barrier, inc=1, device_id={"tp": lax.rem(tp + d, n_tp)}, device_id_type=MESH
        )
    acc_rope[...] = jnp.zeros_like(acc_rope)
    acc_q[...] = jnp.zeros_like(acc_q)
    pl.semaphore_wait(barrier, n_sp + n_tp - 2)
    loads[0].wait()

    def remote(src, dst, send, recv, **where):
        return pltpu.make_async_remote_copy(
            src_ref=src, dst_ref=dst, send_sem=send, recv_sem=recv, device_id=where,
            device_id_type=MESH,
        )

    def chunk(r):
        return pl.ds(pl.multiple_of(r * rc, rc), rc)

    def half(r):
        return pl.ds(pl.multiple_of(r * rc + core * hc, hc), hc)

    def own_copy():
        return remote(tok.at[tp], tok.at[tp], own_tx, own_rx, tp=partner)

    def tok_copy(dy, r):
        to = 2 * lax.rem(yy + dy, n_y) + core
        part = tok.at[tp, chunk(r)]
        return remote(part, part, tok_tx.at[dy, r], tok_rx.at[dy, r], tp=to)

    def fwd_copy(dy, r):
        part = tok.at[2 * lax.rem(yy + n_y - dy, n_y) + core, chunk(r)]
        return remote(part, part, fwd_tx.at[dy, r], fwd_rx.at[dy, r], tp=partner)

    for step in range(CHUNKS):
        for dy in range(1, n_y):
            tok_copy(dy, CHUNKS - 1 - step).start()
    own_copy().start()

    def dot(a, b):
        return jnp.dot(a, b, preferred_element_type=F32)

    def scale_rows(blk, first, count):
        span = min(count, 32)

        def body(i, _):
            at = pl.ds(pl.multiple_of(first + i * span, span), span)
            x = tok[blk, at, :].astype(F32)
            scaled[at, :] = (x * gain[blk]).astype(BF16)
            sq[at, :] += jnp.sum(x * x, axis=1, keepdims=True)
            return 0

        lax.fori_loop(0, count // span, body, 0)

    def project(blk, at, weights):
        k = pl.ds(pl.multiple_of(blk * feats, feats), feats)
        x = scaled[at, :]
        for w, acc in weights:
            n = w.shape[1]
            acc[at, :n] += dot(x, w[k, :])

    early = ((wlat, acc_lat), (wrope, acc_rope))
    late = ((wrec, acc_rec), (wgate, acc_gate), (wq, acc_q))

    sq[...] = jnp.zeros_like(sq)
    acc_lat[...] = jnp.zeros_like(acc_lat)
    acc_rec[...] = jnp.zeros_like(acc_rec)
    acc_gate[...] = jnp.zeros_like(acc_gate)
    for copy in loads[1:17]:
        copy.wait()
    everything = pl.ds(0, rows)

    def own_chip(i, _):
        @pl.when(i == 1)
        def _():
            own_copy().wait()

        blk = 2 * yy + lax.rem(core + i, 2)
        scale_rows(blk, 0, rows)
        project(blk, everything, early + late)
        return 0

    lax.fori_loop(0, 2, own_chip, 0)

    def kvz_copy(dz, r):
        part = kv.at[me, half(r)]
        return remote(part, part, kvz_tx.at[dz, r], kv_rx.at[me, r], sp=me + 2 * dz)

    def kvx_copy(s, r):
        part = kv.at[s, half(r)]
        return remote(part, part, kvx_tx.at[s, r], kv_rx.at[s, r], sp=neighbour)

    def kvd_copy(s, r):
        part = kv.at[s, half(r)]
        return remote(part, part, kvd_tx.at[s, r], kvd_rx.at[s, r], tp=partner)

    def forward_z(r):
        def body(dz, _):
            s = me - 2 * dz
            kvx_copy(s, r).wait_recv()
            kvx_copy(s, r).start()
            kvd_copy(s, r).start()
            return 0

        lax.fori_loop(1, level + 1, body, 0)

    def forward_x(r):
        def body(dz, _):
            s = neighbour - 2 * dz
            kvx_copy(s, r).wait_recv()
            kvd_copy(s, r).start()
            return 0

        lax.fori_loop(1 - column, level + 1, body, 0)

    def tok_step(step, _):
        r = CHUNKS - 1 - step
        at = chunk(r)
        for dy in range(1, n_y):
            tok_copy(dy, r).wait_recv()
            fwd_copy(dy, r).start()
        for dy in range(1, n_y):
            fwd_copy(dy, r).wait_recv()
        for dy in range(1, n_y):
            for b in range(2):
                blk = 2 * lax.rem(yy + n_y - dy, n_y) + b
                scale_rows(blk, r * rc, rc)
                project(blk, at, early + late)
        inverse = lax.rsqrt(sq[at, :] * (1.0 / width) + EPS)
        cosine = cosv[at, :]
        sine = sinv[at, :]
        raw = acc_lat[at, :] * inverse
        norm = raw * lax.rsqrt(jnp.mean(raw * raw, axis=1, keepdims=True) + EPS) * lgain[...]
        kv[me, at, :latent] = norm.astype(BF16)
        kv[me, at, latent:] = rotate(acc_rope[at, :] * inverse, cosine, sine).astype(BF16)
        for dz in range(1, levels):
            @pl.when(level + dz < levels)
            def _():
                kvz_copy(dz, r).start()

        @pl.when(column == 0)
        def _():
            kvx_copy(me, r).start()

        low = (acc_rec[at, :] * inverse).astype(BF16)
        padded[pl.ds(pl.multiple_of(r * rc + 8, 8), rc), :] = low.astype(F32)
        gated[at, :] = gelu_tanh(acc_gate[at, :] * inverse)
        query = acc_q[at, :] * inverse
        total = query.shape[1]
        for h in range(heads):
            start = h * (NOPE + ROPE)
            turned = query if start == 0 else pltpu.roll(query, total - start, 1)
            qcat[h, at, :NOPE] = turned[:, :NOPE].astype(BF16)
            qcat[h, at, NOPE:] = rotate(turned[:, NOPE : NOPE + LANES], cosine, sine).astype(BF16)

        @pl.when(step == 0)
        def _():
            tail_tx[...] = padded[rows : rows + 8, :]

            @pl.when(me + 1 < n_sp)
            def _():
                tail_copy().start()

        @pl.when(step > 0)
        def _():
            forward_z(r + 1)
            forward_x(r + 1)

        return 0

    def tail_copy():
        return remote(tail_tx, tail_rx, tail_s.at[0], tail_s.at[1], sp=me + 1)

    lax.fori_loop(0, CHUNKS, tok_step, 0)

    @pl.when(me > 0)
    def _():
        tail_copy().wait_recv()
        padded[0:8, :] = tail_rx[...]

    @pl.when(me == 0)
    def _():
        padded[0:8, :] = jnp.zeros((8, channels), F32)

    count = taps.shape[0]
    conv = taps[0:1, :] * padded[9 - count : 9 - count + rows, :]
    for k in range(1, count):
        conv = conv + taps[k : k + 1, :] * padded[9 - count + k : 9 - count + k + rows, :]
    low = conv.astype(BF16)
    bw = rmap.shape[1]
    rates, entries = [], []
    for b in range(rmap.shape[0]):
        part = low[:, b * bw : (b + 1) * bw]
        rates.append(dot(part, rmap[b]))
        entries.append(dot(part, imap[b]))
    rate_gate = jax.nn.sigmoid(jnp.concatenate(rates, axis=1))
    entry = jax.nn.sigmoid(jnp.concatenate(entries, axis=1))
    eye = lax.broadcasted_iota(jnp.int32, (rows, rows), 0) == lax.broadcasted_iota(
        jnp.int32, (rows, rows), 1
    )

    def to_column(row):
        return jnp.sum(jnp.where(eye, row, 0.0), axis=1, keepdims=True)

    def to_row(col):
        return jnp.sum(jnp.where(eye, col, 0.0), axis=0, keepdims=True)

    log_keep = -RATE_C * to_column(rate[...]) * rate_gate * softplus(-decay[...])
    a = jnp.exp(log_keep)
    b = jnp.sqrt(one_minus_exp(2.0 * log_keep)) * entry * conv
    row = lax.broadcasted_iota(jnp.int32, (rows, channels), 0)
    d = 1
    while d < rows:
        inside = row >= d
        b = a * jnp.where(inside, pltpu.roll(b, d, 0), 0.0) + b
        a = a * jnp.where(inside, pltpu.roll(a, d, 0), 1.0)
        d *= 2
    a_ref[...] = a
    b_ref[...] = b
    carry_tx[...] = jnp.zeros_like(carry_tx)
    carry_tx[0:1, :] = a[rows - 1 :, :]
    carry_tx[1:2, :] = b[rows - 1 :, :]

    def carry_copy(d):
        return remote(
            carry_tx, carry_rx.at[me], carry_s.at[d], carry_r.at[me], sp=me + d
        )

    def carry_start(d, _):
        carry_copy(d).start()
        return 0

    lax.fori_loop(1, n_sp - me, carry_start, 0)

    forward_z(0)

    root = 1.0 / math.sqrt(NOPE + ROPE)

    def attend(s, diagonal):
        expanded = dot(kv[s, :, :latent], wexp[...]).astype(BF16)
        rope = kv[s, :, latent:]
        for h in range(heads):
            at = h * (NOPE + VDIM)
            keys = jnp.concatenate([expanded[:, at : at + NOPE], rope], axis=1)
            values = expanded[:, at + NOPE : at + NOPE + VDIM]
            scores = lax.dot_general(
                qcat[h], keys, (((1,), (1,)), ((), ())), preferred_element_type=F32
            ) * root
            if diagonal:
                q_at = lax.broadcasted_iota(jnp.int32, scores.shape, 0)
                k_at = lax.broadcasted_iota(jnp.int32, scores.shape, 1)
                scores = jnp.where(k_at <= q_at, scores, -jnp.inf)
                top = jnp.max(scores, axis=1, keepdims=True)
            else:
                old = m_ref[h]
                top = jnp.maximum(old, jnp.max(scores, axis=1, keepdims=True))
                shrink = jnp.exp(old - top)
            weights = jnp.exp(scores - top)
            total = jnp.sum(weights, axis=1, keepdims=True)
            mixed_values = dot(weights.astype(BF16), values)
            m_ref[h] = top
            if diagonal:
                l_ref[h] = total
                o_ref[h] = mixed_values
            else:
                l_ref[h] = l_ref[h] * shrink + total
                o_ref[h] = o_ref[h] * shrink + mixed_values

    for copy in loads[17:]:
        copy.wait()
    attend(me, True)
    forward_x(0)

    def earlier(j, _):
        s = me - j
        for r in range(CHUNKS):
            kvd_copy(s, r).wait_recv()
        attend(s, False)
        return 0

    lax.fori_loop(1, me + 1, earlier, 0)

    def join(s, carried):
        remote(carry_tx, carry_rx.at[s], carry_s.at[0], carry_r.at[s], sp=neighbour).wait_recv()
        return carry_rx[s, 0:1, :] * carried + carry_rx[s, 1:2, :]

    carried = lax.fori_loop(0, me, join, jnp.zeros((1, channels), F32))
    rec_out = (b_ref[...] + a_ref[...] * carried) * gated[...]
    rb[...] = (rec_out * rgain[...]).astype(BF16)
    sq_tx[...] = jnp.zeros_like(sq_tx)
    sq_tx[0:1, :] = to_row(jnp.sum(rec_out * rec_out, axis=1, keepdims=True))
    att_sq = jnp.zeros((rows, 1), F32)
    for h in range(heads):
        att = o_ref[h] / l_ref[h]
        att_sq = att_sq + jnp.sum(att * att, axis=1, keepdims=True)
        at = slice(h * VDIM, (h + 1) * VDIM)
        ab[:, at] = (att * again[:, at]).astype(BF16)
    sq_tx[1:2, :] = to_row(att_sq)

    def sq_copy(d):
        return remote(
            sq_tx, sq_rx.at[d], sq_s.at[d], sq_r.at[d], tp=lax.rem(tp + d, n_tp)
        )

    for d in range(1, n_tp):
        sq_copy(d).start()
    sums = sq_tx[...]
    for d in range(1, n_tp):
        sq_copy(d).wait_recv()
        sums = sums + sq_rx[d]
    scale = lax.rsqrt(sums * (1.0 / (channels * n_tp)) + EPS)
    inv_r[...] = to_column(scale[0:1, :])
    scale = lax.rsqrt(sums * (1.0 / (heads * VDIM * n_tp)) + EPS)
    inv_a[...] = to_column(scale[1:2, :])

    def d2d_copy(dy, c):
        return remote(
            d2d_tx.at[dy, c], d2d_rx.at[dy, c], d2d_s.at[dy, c], d2d_r.at[dy, c], tp=partner
        )

    def y_copy(dy, c):
        to = 2 * lax.rem(yy + dy, n_y) + core
        return remote(y_tx.at[dy, c], y_rx.at[dy, c], y_s.at[dy, c], y_r.at[dy, c], tp=to)

    def produce(dy, c):
        first = pl.multiple_of(2 * rd * lax.rem(yy + dy, n_y), 2 * rd)
        at = pl.ds(first, 2 * rd)
        cols = pl.ds(pl.multiple_of(c * cb, cb), cb)
        pr[...] = dot(rb[at, :], wor[:, cols]) * inv_r[at, :] + dot(
            ab[at, :], woa[:, cols]
        ) * inv_a[at, :]
        theirs = pl.ds(pl.multiple_of((1 - core) * rd, rd), rd)
        mine = pl.ds(pl.multiple_of(core * rd, rd), rd)
        d2d_tx[dy, c] = pr[theirs, :].astype(BF16)
        d2d_copy(dy, c).start()
        comb[dy, c] = pr[mine, :]

    def send_pair(dy, c):
        d2d_copy(dy, c).wait_recv()
        y_tx[dy, c] = (comb[dy, c] + d2d_rx[dy, c].astype(F32)).astype(BF16)
        y_copy(dy, c).start()

    for dy in range(1, n_y):
        def away(c, _):
            @pl.when(c < COLS)
            def _():
                produce(dy, c)

            @pl.when(c > 0)
            def _():
                send_pair(dy, c - 1)

            return 0

        lax.fori_loop(0, COLS + 1, away, 0)

    def home(c, _):
        produce(0, c)
        return 0

    lax.fori_loop(0, COLS, home, 0)

    def gather(c, total):
        d2d_copy(0, c).wait_recv()
        value = comb[0, c] + d2d_rx[0, c].astype(F32)
        for dy in range(1, n_y):
            y_copy(dy, c).wait_recv()
            value = value + y_rx[dy, c].astype(F32)
        mixed[c] = value
        return total + jnp.sum(value * value, axis=1, keepdims=True)

    total = lax.fori_loop(0, COLS, gather, jnp.zeros((rd, 1), F32))
    last = lax.rsqrt(total * (1.0 / width) + EPS)

    for c in range(COLS):
        at = slice(c * cb, (c + 1) * cb)
        out_ref[:, at] = (mixed[c] * last * pgain[:, at]).astype(BF16)

    def drain(r, _):
        for dy in range(1, n_y):
            tok_copy(dy, r).wait_send()
            fwd_copy(dy, r).wait_send()
        for dz in range(1, levels):
            @pl.when(level + dz < levels)
            def _():
                kvz_copy(dz, r).wait_send()

        @pl.when(column == 0)
        def _():
            kvx_copy(me, r).wait_send()

        def sent_z(dz, _):
            kvx_copy(me - 2 * dz, r).wait_send()
            kvd_copy(me - 2 * dz, r).wait_send()
            return 0

        lax.fori_loop(1, level + 1, sent_z, 0)

        def sent_x(dz, _):
            kvd_copy(neighbour - 2 * dz, r).wait_send()
            return 0

        lax.fori_loop(1 - column, level + 1, sent_x, 0)
        return 0

    lax.fori_loop(0, CHUNKS, drain, 0)

    @pl.when(me + 1 < n_sp)
    def _():
        tail_copy().wait_send()

    def carry_done(d, _):
        carry_copy(d).wait_send()
        return 0

    lax.fori_loop(1, n_sp - me, carry_done, 0)
    for d in range(1, n_tp):
        sq_copy(d).wait_send()

    def sums_done(c, _):
        for dy in range(n_y):
            d2d_copy(dy, c).wait_send()
            if dy > 0:
                y_copy(dy, c).wait_send()
        return 0

    lax.fori_loop(0, COLS, sums_done, 0)


def shards(
    tokens, pre_gain, rate_factor, w_rec_in, w_rec_gate, conv_taps, rate_maps, input_maps,
    decay_param, w_query, w_latent, w_rope_key, latent_gain, w_expand, rec_gain, att_gain,
    w_out_rec, w_out_att, post_gain,
):
    n_sp = lax.axis_size("sp")
    n_tp = lax.axis_size("tp")
    n_y = n_tp // 2
    rows, feats = tokens.shape
    width = feats * n_tp
    channels = w_rec_in.shape[1]
    latent = w_latent.shape[1]
    q_cols = w_query.shape[1]
    heads = q_cols // (NOPE + ROPE)
    q_pad = -(-q_cols // LANES) * LANES
    rd = rows // n_tp
    cb = width // COLS

    lane = jnp.arange(LANES)
    frequency = 1.0 / THETA ** ((2 * (lane % (ROPE // 2))).astype(F32) / ROPE)
    places = (lax.axis_index("sp") * rows + jnp.arange(rows)).astype(F32)
    turned = places[:, None] * frequency[None, :]
    cosine = jnp.where(lane < ROPE, jnp.cos(turned), 0.0)
    sine = jnp.sin(turned) * jnp.where(lane < ROPE // 2, -1.0, jnp.where(lane < ROPE, 1.0, 0.0))

    def row(v):
        return v.reshape(1, -1)

    args = (
        tokens, pre_gain.reshape(n_tp, 1, feats), row(rate_factor), w_rec_in, w_rec_gate,
        conv_taps, rate_maps, input_maps, row(decay_param), w_query, w_latent, w_rope_key,
        row(latent_gain), w_expand, row(rec_gain), row(att_gain), w_out_rec, w_out_att,
        row(post_gain), cosine, sine,
    )
    vm = pltpu.VMEM
    dma = pltpu.SemaphoreType.DMA

    def like(x):
        return vm(x.shape, x.dtype)

    scratch = [
        vm((n_tp, rows, feats), BF16), vm((rows, feats), BF16), like(args[1]), like(args[2]),
        like(args[3]), like(args[4]), like(args[5]), like(args[6]), like(args[7]), like(args[8]),
        like(args[9]), like(args[10]), like(args[11]), like(args[12]), like(args[13]),
        like(args[14]), like(args[15]), like(args[16]), like(args[17]), like(args[18]),
        like(args[19]), like(args[20]),
        vm((rows, latent), F32), vm((rows, LANES), F32), vm((rows, channels), F32),
        vm((rows, channels), F32), vm((rows, q_pad), F32), vm((rows, 1), F32),
        vm((n_sp, rows, latent + LANES), BF16), vm((heads, rows, NOPE + LANES), BF16),
        vm((rows + 8, channels), F32), vm((rows, channels), F32),
        vm((heads, rows, 1), F32), vm((heads, rows, 1), F32), vm((heads, rows, VDIM), F32),
        vm((rows, channels), F32), vm((rows, channels), F32),
        vm((rows, channels), BF16), vm((rows, heads * VDIM), BF16),
        vm((8, channels), F32), vm((8, channels), F32), vm((8, channels), F32),
        vm((n_sp, 8, channels), F32), vm((8, rows), F32), vm((n_tp, 8, rows), F32),
        vm((rows, 1), F32), vm((rows, 1), F32),
        vm((2 * rd, cb), F32), vm((n_y, COLS, rd, cb), F32), vm((n_y, COLS, rd, cb), BF16),
        vm((n_y, COLS, rd, cb), BF16), vm((n_y, COLS, rd, cb), BF16),
        vm((n_y, COLS, rd, cb), BF16), vm((COLS, rd, cb), F32),
        dma((len(args),)), dma, dma, dma((n_y, CHUNKS)), dma((n_y, CHUNKS)),
        dma((n_y, CHUNKS)), dma((n_y, CHUNKS)),
        dma((n_sp // 2, CHUNKS)), dma((n_sp, CHUNKS)), dma((n_sp, CHUNKS)),
        dma((n_sp, CHUNKS)), dma((n_sp, CHUNKS)),
        dma((2,)), dma((n_sp,)), dma((n_sp,)), dma((n_tp,)), dma((n_tp,)),
        dma((n_y, COLS)), dma((n_y, COLS)), dma((n_y, COLS)), dma((n_y, COLS)),
    ]
    return pl.pallas_call(
        functools.partial(fused_kernel, n_sp, n_tp, heads),
        out_shape=jax.ShapeDtypeStruct((rd, width), BF16),
        in_specs=[pl.BlockSpec(memory_space=pl.ANY)] * len(args),
        out_specs=pl.BlockSpec(memory_space=pltpu.VMEM),
        scratch_shapes=scratch,
        compiler_params=pltpu.CompilerParams(
            collective_id=0, has_side_effects=True, vmem_limit_bytes=67043328
        ),
        name="layer",
    )(*args)


def solution(mesh):
    placed = (
        P("sp", "tp"),
        P(),
        P("sp"),
        P(None, "tp"),
        P(None, "tp"),
        P(None, "tp"),
        P("tp", None, None),
        P("tp", None, None),
        P("tp"),
        P(None, "tp"),
        P(),
        P(),
        P(),
        P(None, "tp"),
        P("tp"),
        P("tp"),
        P("tp", None),
        P("tp", None),
        P(),
    )
    return jax.shard_map(
        shards, mesh=mesh, in_specs=placed, out_specs=P(("sp", "tp"), None), check_vma=False
    )
```

time: 181 us -> 80.3 us (0.44)
  the two profiles are of different devices: /device:TPU:24 before, /device:TPU:30 now
where the time goes in v1:
time: 80.3 us; the launch traced here: 80.1 us
  Pallas kernels  74.6 us (93%)
  local copies, waits for them, and re-layouts  4.23 us (5%)
  other arithmetic  1.26 us (2%)
    pallas_call x1, Pallas kernels, shards(): pl.pallas_call(functools.partial(fused_kernel, n_sp, n_tp, heads), out_sh...  74.6 us
    unnamed x2, local copies, waits for them, and re-layouts  4.23 us

profile of v1, /device:TPU:30, one launch (start us, length us, event | category | flops | bytes accessed | tf_op | source)
XLA Modules:
  0.0 80.1 jit_solution(14210270864430823365)
XLA Ops:
  0.0 1.2 %fusion.1 = (f32[256,128]{1,0:T(8,128)}, f32[256,128]{1,0:T(8,128)}) fusion(f32[128]{0:T(128)S(1)} %get-tuple-element.7, f32[128]{0:T(128)S(1)} %get-tuple-element.8, f32[256]{0:T(256)S(1)} %add_convert_fusion, pred[128]{0:T(512)(128)(4,1)S(1)} %iota_compare_fusion), kind=kLoop, calls=%fused_computation.3 | loop fusion | flops 98304 | bytes 264320 | tf_op jit(solution)/shard_map/mul | solution.py:560
  1.3 2.4 %copy.20.w_rope = bf16[4096,64]{1,0:T(8,128)(2,1)} copy(bf16[4096,64]{0,1:T(8,128)(2,1)} %param.30) | data formatting | bytes 1048576 | tf_op args[11]
  3.6 74.6 %layer.1 = bf16[64,4096]{1,0:T(8,128)(2,1)} custom-call(bf16[256,1024]{1,0:T(8,128)(2,1)} %tokens.1, f32[4,1,1024]{2,1,0:T(1,128)} %bitcast.7, f32[1,256]{1,0:T(1,128)} %bitcast.10, bf16[4096,256]{1,0:T(8,128)(2,1)} %w_rec.1, bf16[4096,256]{1,0:T(8,128)(2,1)} %w_gate.1, f32[4,256]{1,0:T(4,128)} %taps_in.1, bf16[2,128,128]{2,1,0:T(8,128)(2,1)} %rmap_in.1, ...), custom_call_target="tpu_custom_call" | custom-call | tf_op jit(solution)/shard_map/layer/pallas_call | solution.py:603
  78.3 1.9 %copy.22 = bf16[64,4096]{1,0:T(8,128)(2,1)} copy(bf16[64,4096]{1,0:T(8,128)(2,1)} %layer.1) | data formatting | bytes 1048576
  (3 shorter events, 0.0 us)

commit v2 on v1

--- a/solution.py
+++ b/solution.py
@@ -3,6 +3,7 @@
 
 import jax
 import jax.numpy as jnp
+import numpy as np
 from jax import lax
 from jax.experimental import pallas as pl
 from jax.experimental.pallas import tpu as pltpu
@@ -17,6 +18,7 @@
 RATE_C = 8.0
 THETA = 10000.0
 CHUNKS = 4
+BATCH = 4
 COLS = 4
 
 MESH = pl.DeviceIdType.MESH
@@ -59,15 +61,15 @@
     n_sp, n_tp, heads,
     tokens, pre_gain, rate_factor, w_rec, w_gate, taps_in, rmap_in, imap_in, decay_in, w_query,
     w_latent, w_rope, lat_gain_in, w_expand, rec_gain_in, att_gain_in, w_or, w_oa, post_gain_in,
-    cos_in, sin_in,
+    turns_in, starts_in,
     out_ref,
     tok, scaled, gain, rate, wrec, wgate, taps, rmap, imap, decay, wq, wlat, wrope, lgain, wexp,
-    rgain, again, wor, woa, pgain, cosv, sinv,
+    rgain, again, wor, woa, pgain, turns, starts,
     acc_lat, acc_rope, acc_rec, acc_gate, acc_q, sq, kv, qcat, padded, gated,
     m_ref, l_ref, o_ref, a_ref, b_ref, rb, ab,
-    tail_tx, tail_rx, carry_tx, carry_rx, sq_tx, sq_rx, inv_r, inv_a,
-    pr, comb, d2d_tx, d2d_rx, y_tx, y_rx, mixed,
-    load_sem, own_tx, own_rx, tok_tx, tok_rx, fwd_tx, fwd_rx,
+    tail_tx, tail_rx, carry_tx, carry_rx, sq_tx, sq_rx, inv,
+    prod, d2d_tx, d2d_rx, y_tx, y_rx, mixed,
+    load_sem, weight_sem, own_tx, own_rx, tok_tx, tok_rx, fwd_tx, fwd_rx,
     kvz_tx, kvx_tx, kv_rx, kvd_tx, kvd_rx,
     tail_s, carry_s, carry_r, sq_s, sq_r, d2d_s, d2d_r, y_s, y_r,
 ):
@@ -90,16 +92,40 @@
     rd = rows // n_tp
     cb = width // COLS
 
-    pairs = (
-        (tokens, tok.at[tp]), (pre_gain, gain), (w_latent, wlat), (w_rope, wrope), (w_rec, wrec),
-        (w_gate, wgate), (w_query, wq), (lat_gain_in, lgain), (cos_in, cosv), (sin_in, sinv),
-        (rate_factor, rate), (taps_in, taps), (rmap_in, rmap), (imap_in, imap), (decay_in, decay),
-        (rec_gain_in, rgain), (att_gain_in, again), (w_expand, wexp), (w_or, wor), (w_oa, woa),
+    small = (
+        (tokens, tok.at[tp]), (pre_gain, gain), (lat_gain_in, lgain), (turns_in, turns),
+        (starts_in, starts),
+    )
+    later = (
+        (w_expand, wexp), (rate_factor, rate), (taps_in, taps), (rmap_in, rmap), (imap_in, imap),
+        (decay_in, decay), (rec_gain_in, rgain), (att_gain_in, again), (w_or, wor), (w_oa, woa),
         (post_gain_in, pgain),
     )
-    loads = [pltpu.make_async_copy(s, d, load_sem.at[i]) for i, (s, d) in enumerate(pairs)]
-    for copy in loads:
+    projections = ((w_latent, wlat), (w_rec, wrec), (w_gate, wgate), (w_query, wq))
+
+    def loads_of(group, first):
+        return [
+            pltpu.make_async_copy(s, d, load_sem.at[first + i]) for i, (s, d) in enumerate(group)
+        ]
+
+    def features(blk):
+        return pl.ds(pl.multiple_of(blk * feats, feats), feats)
+
+    def weight_loads(blk):
+        at = features(blk)
+        copies = [pltpu.make_async_copy(w_rope.at[:, at], wrope.at[:, at], weight_sem.at[0, blk])]
+        for i, (s, d) in enumerate(projections):
+            copies.append(pltpu.make_async_copy(s.at[at], d.at[at], weight_sem.at[1 + i, blk]))
+        return copies
+
+    first_loads = loads_of(small, 0)
+    last_loads = loads_of(later, len(small))
+    for copy in first_loads:
         copy.start()
+    for dy in range(n_y):
+        for b in range(2):
+            for copy in weight_loads(2 * lax.rem(yy + dy, n_y) + lax.rem(core + b, 2)):
+                copy.start()
 
     barrier = pltpu.get_barrier_semaphore()
     for d in range(1, n_sp):
@@ -110,10 +136,17 @@
         pl.semaphore_signal(
             barrier, inc=1, device_id={"tp": lax.rem(tp + d, n_tp)}, device_id_type=MESH
         )
-    acc_rope[...] = jnp.zeros_like(acc_rope)
-    acc_q[...] = jnp.zeros_like(acc_q)
-    pl.semaphore_wait(barrier, n_sp + n_tp - 2)
-    loads[0].wait()
+    with jax.named_scope("entry"):
+        for ref in (acc_lat, acc_rope, acc_rec, acc_gate, acc_q, sq):
+            ref[...] = jnp.zeros_like(ref)
+
+        def blank(s, _):
+            kv[s] = jnp.zeros(kv.shape[1:], BF16)
+            return 0
+
+        lax.fori_loop(me + 1, lax.div(me + BATCH - 1, BATCH) * BATCH, blank, 0)
+        pl.semaphore_wait(barrier, n_sp + n_tp - 2)
+        first_loads[0].wait()
 
     def remote(src, dst, send, recv, **where):
         return pltpu.make_async_remote_copy(
@@ -147,6 +180,16 @@
     def dot(a, b):
         return jnp.dot(a, b, preferred_element_type=F32)
 
+    def dot_t(a, b):
+        return lax.dot_general(a, b, (((1,), (1,)), ((), ())), preferred_element_type=F32)
+
+    def tiles(x):
+        return [x[:, i : i + LANES] for i in range(0, x.shape[1], LANES)]
+
+    def wide(x, count):
+        return jnp.concatenate([x] * count, axis=1) if count > 1 else x
+
+    @jax.named_scope("scale")
     def scale_rows(blk, first, count):
         span = min(count, 32)
 
@@ -154,40 +197,47 @@
             at = pl.ds(pl.multiple_of(first + i * span, span), span)
             x = tok[blk, at, :].astype(F32)
             scaled[at, :] = (x * gain[blk]).astype(BF16)
-            sq[at, :] += jnp.sum(x * x, axis=1, keepdims=True)
+            sq[at, :] += functools.reduce(jnp.add, tiles(x * x))
             return 0
 
         lax.fori_loop(0, count // span, body, 0)
 
-    def project(blk, at, weights):
-        k = pl.ds(pl.multiple_of(blk * feats, feats), feats)
+    @jax.named_scope("early")
+    def project_early(blk, at):
+        k = features(blk)
         x = scaled[at, :]
-        for w, acc in weights:
-            n = w.shape[1]
-            acc[at, :n] += dot(x, w[k, :])
-
-    early = ((wlat, acc_lat), (wrope, acc_rope))
-    late = ((wrec, acc_rec), (wgate, acc_gate), (wq, acc_q))
-
-    sq[...] = jnp.zeros_like(sq)
-    acc_lat[...] = jnp.zeros_like(acc_lat)
-    acc_rec[...] = jnp.zeros_like(acc_rec)
-    acc_gate[...] = jnp.zeros_like(acc_gate)
-    for copy in loads[1:17]:
+        acc_rope[at, : wrope.shape[0]] += dot_t(x, wrope[:, k])
+        acc_lat[at, :] += dot(x, wlat[k, :])
+
+    @jax.named_scope("late")
+    def project_late(blk, at):
+        k = features(blk)
+        x = scaled[at, :]
+        for w, acc in ((wrec, acc_rec), (wgate, acc_gate), (wq, acc_q)):
+            acc[at, : w.shape[1]] += dot(x, w[k, :])
+
+    for copy in first_loads[1:]:
         copy.wait()
     everything = pl.ds(0, rows)
 
     def own_chip(i, _):
+        blk = 2 * yy + lax.rem(core + i, 2)
+
         @pl.when(i == 1)
         def _():
             own_copy().wait()
 
-        blk = 2 * yy + lax.rem(core + i, 2)
         scale_rows(blk, 0, rows)
-        project(blk, everything, early + late)
+        with jax.named_scope("weights"):
+            for copy in weight_loads(blk):
+                copy.wait()
+        project_early(blk, everything)
+        project_late(blk, everything)
         return 0
 
     lax.fori_loop(0, 2, own_chip, 0)
+    for copy in last_loads:
+        copy.start()
 
     def kvz_copy(dz, r):
         part = kv.at[me, half(r)]
@@ -201,7 +251,8 @@
         part = kv.at[s, half(r)]
         return remote(part, part, kvd_tx.at[s, r], kvd_rx.at[s, r], tp=partner)
 
-    def forward_z(r):
+    @jax.named_scope("fwdz")
+    def forward_z(r, near, far):
         def body(dz, _):
             s = me - 2 * dz
             kvx_copy(s, r).wait_recv()
@@ -209,8 +260,9 @@
             kvd_copy(s, r).start()
             return 0
 
-        lax.fori_loop(1, level + 1, body, 0)
-
+        lax.fori_loop(near, jnp.minimum(far, level + 1), body, 0)
+
+    @jax.named_scope("fwdx")
     def forward_x(r):
         def body(dz, _):
             s = neighbour - 2 * dz
@@ -220,22 +272,22 @@
 
         lax.fori_loop(1 - column, level + 1, body, 0)
 
-    def tok_step(step, _):
-        r = CHUNKS - 1 - step
-        at = chunk(r)
-        for dy in range(1, n_y):
-            tok_copy(dy, r).wait_recv()
-            fwd_copy(dy, r).start()
-        for dy in range(1, n_y):
-            fwd_copy(dy, r).wait_recv()
-        for dy in range(1, n_y):
-            for b in range(2):
-                blk = 2 * lax.rem(yy + n_y - dy, n_y) + b
-                scale_rows(blk, r * rc, rc)
-                project(blk, at, early + late)
-        inverse = lax.rsqrt(sq[at, :] * (1.0 / width) + EPS)
-        cosine = cosv[at, :]
-        sine = sinv[at, :]
+    def angles(at):
+        lane = lax.broadcasted_iota(jnp.int32, (1, LANES), 1)
+        kept = jnp.where(lane < ROPE, 1.0, 0.0)
+        sign = jnp.where(lane < ROPE // 2, -1.0, kept)
+        c, s = turns[0, at, :], turns[1, at, :]
+        c0, s0 = starts[0, me], starts[1, me]
+        return (c * c0 - s * s0) * kept, (s * c0 + c * s0) * sign
+
+    def inverse_of(at):
+        total = jnp.sum(sq[at, :], axis=1, keepdims=True)
+        return lax.rsqrt(total * (1.0 / width) + EPS)
+
+    @jax.named_scope("latent")
+    def finish_latent(r, at):
+        inverse = inverse_of(at)
+        cosine, sine = angles(at)
         raw = acc_lat[at, :] * inverse
         norm = raw * lax.rsqrt(jnp.mean(raw * raw, axis=1, keepdims=True) + EPS) * lgain[...]
         kv[me, at, :latent] = norm.astype(BF16)
@@ -249,16 +301,45 @@
         def _():
             kvx_copy(me, r).start()
 
-        low = (acc_rec[at, :] * inverse).astype(BF16)
-        padded[pl.ds(pl.multiple_of(r * rc + 8, 8), rc), :] = low.astype(F32)
-        gated[at, :] = gelu_tanh(acc_gate[at, :] * inverse)
-        query = acc_q[at, :] * inverse
-        total = query.shape[1]
-        for h in range(heads):
-            start = h * (NOPE + ROPE)
-            turned = query if start == 0 else pltpu.roll(query, total - start, 1)
-            qcat[h, at, :NOPE] = turned[:, :NOPE].astype(BF16)
-            qcat[h, at, NOPE:] = rotate(turned[:, NOPE : NOPE + LANES], cosine, sine).astype(BF16)
+    def tok_step(step, _):
+        r = CHUNKS - 1 - step
+        at = chunk(r)
+        with jax.named_scope("tokwait"):
+            for dy in range(1, n_y):
+                tok_copy(dy, r).wait_recv()
+                fwd_copy(dy, r).start()
+
+        for b in range(2):
+            for dy in range(1, n_y):
+                blk = 2 * lax.rem(yy + n_y - dy, n_y) + lax.rem(core + b, 2)
+                if b == 1:
+                    with jax.named_scope("fwdwait"):
+                        fwd_copy(dy, r).wait_recv()
+                scale_rows(blk, r * rc, rc)
+
+                @pl.when(step == 0)
+                def _():
+                    for copy in weight_loads(blk):
+                        copy.wait()
+
+                project_early(blk, at)
+                if b == 1 and dy == n_y - 1:
+                    finish_latent(r, at)
+                project_late(blk, at)
+
+        with jax.named_scope("finish"):
+            inverse = inverse_of(at)
+            cosine, sine = angles(at)
+            low = (acc_rec[at, :] * inverse).astype(BF16)
+            padded[pl.ds(pl.multiple_of(r * rc + 8, 8), rc), :] = low.astype(F32)
+            gated[at, :] = gelu_tanh(acc_gate[at, :] * inverse)
+            query = acc_q[at, :] * inverse
+            total = query.shape[1]
+            for h in range(heads):
+                start = h * (NOPE + ROPE)
+                turned = query if start == 0 else pltpu.roll(query, total - start, 1)
+                qcat[h, at, :NOPE] = turned[:, :NOPE].astype(BF16)
+                qcat[h, at, NOPE:] = rotate(turned[:, NOPE : NOPE + LANES], cosine, sine).astype(BF16)
 
         @pl.when(step == 0)
         def _():
@@ -270,8 +351,11 @@
 
         @pl.when(step > 0)
         def _():
-            forward_z(r + 1)
-            forward_x(r + 1)
+            forward_z(r + 1, 1, 2)
+
+        @pl.when(step > 1)
+        def _():
+            forward_z(r + 2, 2, levels)
 
         return 0
 
@@ -279,6 +363,9 @@
         return remote(tail_tx, tail_rx, tail_s.at[0], tail_s.at[1], sp=me + 1)
 
     lax.fori_loop(0, CHUNKS, tok_step, 0)
+
+    for copy in last_loads:
+        copy.wait()
 
     @pl.when(me > 0)
     def _():
@@ -289,6 +376,8 @@
     def _():
         padded[0:8, :] = jnp.zeros((8, channels), F32)
 
+    mark = jax.named_scope("rec")
+    mark.__enter__()
     count = taps.shape[0]
     conv = taps[0:1, :] * padded[9 - count : 9 - count + rows, :]
     for k in range(1, count):
@@ -328,6 +417,8 @@
     carry_tx[0:1, :] = a[rows - 1 :, :]
     carry_tx[1:2, :] = b[rows - 1 :, :]
 
+    mark.__exit__(None, None, None)
+
     def carry_copy(d):
         return remote(
             carry_tx, carry_rx.at[me], carry_s.at[d], carry_r.at[me], sp=me + d
@@ -339,86 +430,138 @@
 
     lax.fori_loop(1, n_sp - me, carry_start, 0)
 
-    forward_z(0)
+    forward_z(0, 1, 2)
+    forward_z(1, 2, levels)
 
     root = 1.0 / math.sqrt(NOPE + ROPE)
 
-    def attend(s, diagonal):
-        expanded = dot(kv[s, :, :latent], wexp[...]).astype(BF16)
-        rope = kv[s, :, latent:]
+    @jax.named_scope("attend")
+    def attend(keys_latent, keys_rope, limit):
+        expanded = dot(keys_latent, wexp[...]).astype(BF16)
         for h in range(heads):
             at = h * (NOPE + VDIM)
-            keys = jnp.concatenate([expanded[:, at : at + NOPE], rope], axis=1)
+            keys = jnp.concatenate([expanded[:, at : at + NOPE], keys_rope], axis=1)
             values = expanded[:, at + NOPE : at + NOPE + VDIM]
-            scores = lax.dot_general(
-                qcat[h], keys, (((1,), (1,)), ((), ())), preferred_element_type=F32
-            ) * root
-            if diagonal:
-                q_at = lax.broadcasted_iota(jnp.int32, scores.shape, 0)
-                k_at = lax.broadcasted_iota(jnp.int32, scores.shape, 1)
-                scores = jnp.where(k_at <= q_at, scores, -jnp.inf)
-                top = jnp.max(scores, axis=1, keepdims=True)
+            scores = dot_t(qcat[h], keys) * root
+            k_at = lax.broadcasted_iota(jnp.int32, scores.shape, 1)
+            if limit is None:
+                limit_at = lax.broadcasted_iota(jnp.int32, scores.shape, 0) + 1
             else:
+                limit_at = limit
+            scores = tiles(jnp.where(k_at < limit_at, scores, -jnp.inf))
+            top = jnp.max(functools.reduce(jnp.maximum, scores), axis=1, keepdims=True)
+            if limit is not None:
                 old = m_ref[h]
-                top = jnp.maximum(old, jnp.max(scores, axis=1, keepdims=True))
+                top = jnp.maximum(old, top)
                 shrink = jnp.exp(old - top)
-            weights = jnp.exp(scores - top)
-            total = jnp.sum(weights, axis=1, keepdims=True)
-            mixed_values = dot(weights.astype(BF16), values)
-            m_ref[h] = top
-            if diagonal:
-                l_ref[h] = total
-                o_ref[h] = mixed_values
-            else:
-                l_ref[h] = l_ref[h] * shrink + total
-                o_ref[h] = o_ref[h] * shrink + mixed_values
-
-    for copy in loads[17:]:
-        copy.wait()
-    attend(me, True)
+            weights = [jnp.exp(x - top) for x in scores]
+            total = functools.reduce(jnp.add, weights)
+            found = dot(jnp.concatenate([x.astype(BF16) for x in weights], axis=1), values)
+            if limit is not None:
+                total = total + l_ref[h] * shrink
+                found = found + o_ref[h] * shrink
+            m_ref[h] = jnp.broadcast_to(top, m_ref.shape[1:])
+            l_ref[h] = total
+            o_ref[h] = found
+
+    def attend_chunk(r):
+        def ready(s, _):
+            kvd_copy(s, r).wait_recv()
+            return 0
+
+        with jax.named_scope("kvwait"):
+            lax.fori_loop(0, me, ready, 0)
+
+        def group(g, _):
+            several = pl.ds(g * BATCH, BATCH)
+            count = BATCH * rc
+            attend(
+                kv[several, chunk(r), :latent].reshape(count, latent),
+                kv[several, chunk(r), latent:].reshape(count, LANES),
+                (me - g * BATCH) * rc,
+            )
+            return 0
+
+        lax.fori_loop(0, lax.div(me + BATCH - 1, BATCH), group, 0)
+
+    attend(kv[me, :, :latent], kv[me, :, latent:], None)
+    forward_z(0, 2, levels)
+
+    def sq_copy(kind, d):
+        return remote(
+            sq_tx.at[kind], sq_rx.at[kind, d], sq_s.at[kind, d], sq_r.at[kind, d],
+            tp=lax.rem(tp + d, n_tp),
+        )
+
+    def share_squares(kind, column):
+        sq_tx[kind] = jnp.broadcast_to(to_row(column), sq_tx.shape[1:])
+        for d in range(1, n_tp):
+            sq_copy(kind, d).start()
+
+    @jax.named_scope("sums")
+    def join_squares(kind, count):
+        total = sq_tx[kind]
+        for d in range(1, n_tp):
+            sq_copy(kind, d).wait_recv()
+            total = total + sq_rx[kind, d]
+        scale = lax.rsqrt(total * (1.0 / count) + EPS)
+        inv[kind] = jnp.broadcast_to(to_column(scale[0:1, :]), inv.shape[1:])
+
+    @jax.named_scope("join")
+    def finish_recurrence():
+        def join(s, carried):
+            remote(
+                carry_tx, carry_rx.at[s], carry_s.at[0], carry_r.at[s], sp=neighbour
+            ).wait_recv()
+            return carry_rx[s, 0:1, :] * carried + carry_rx[s, 1:2, :]
+
+        carried = lax.fori_loop(0, me, join, jnp.zeros((1, channels), F32))
+        rec_out = (b_ref[...] + a_ref[...] * carried) * gated[...]
+        rb[...] = (rec_out * rgain[...]).astype(BF16)
+        share_squares(0, jnp.sum(rec_out * rec_out, axis=1, keepdims=True))
+
+    def block(dy):
+        return pl.ds(pl.multiple_of(2 * rd * lax.rem(yy + dy, n_y), 2 * rd), 2 * rd)
+
+    def cols(c):
+        return pl.ds(pl.multiple_of(c * cb, cb), cb)
+
+    @jax.named_scope("recprod")
+    def multiply(dy, c, left, right, add):
+        at = block(dy)
+        value = dot(left[at, :], right[:, cols(c)])
+        if add:
+            count = cb // LANES
+            value = value * wide(inv[1, at, :], count) + prod[dy, c] * wide(inv[0, at, :], count)
+        prod[dy, c] = value
+
+    forward_x(CHUNKS - 1)
+    forward_x(CHUNKS - 2)
+    attend_chunk(CHUNKS - 1)
+    for r in range(CHUNKS - 3, 0, -1):
+        forward_x(r)
+        attend_chunk(r + 1)
+    finish_recurrence()
+    attend_chunk(1)
     forward_x(0)
 
-    def earlier(j, _):
-        s = me - j
-        for r in range(CHUNKS):
-            kvd_copy(s, r).wait_recv()
-        attend(s, False)
-        return 0
-
-    lax.fori_loop(1, me + 1, earlier, 0)
-
-    def join(s, carried):
-        remote(carry_tx, carry_rx.at[s], carry_s.at[0], carry_r.at[s], sp=neighbour).wait_recv()
-        return carry_rx[s, 0:1, :] * carried + carry_rx[s, 1:2, :]
-
-    carried = lax.fori_loop(0, me, join, jnp.zeros((1, channels), F32))
-    rec_out = (b_ref[...] + a_ref[...] * carried) * gated[...]
-    rb[...] = (rec_out * rgain[...]).astype(BF16)
-    sq_tx[...] = jnp.zeros_like(sq_tx)
-    sq_tx[0:1, :] = to_row(jnp.sum(rec_out * rec_out, axis=1, keepdims=True))
+    for dy in range(n_y):
+        def rec_product(c, _):
+            multiply(dy, c, rb, wor, False)
+            return 0
+
+        lax.fori_loop(0, COLS, rec_product, 0)
+    join_squares(0, channels * n_tp)
+    attend_chunk(0)
+
     att_sq = jnp.zeros((rows, 1), F32)
     for h in range(heads):
-        att = o_ref[h] / l_ref[h]
+        att = o_ref[h] / jnp.sum(l_ref[h], axis=1, keepdims=True)
         att_sq = att_sq + jnp.sum(att * att, axis=1, keepdims=True)
         at = slice(h * VDIM, (h + 1) * VDIM)
         ab[:, at] = (att * again[:, at]).astype(BF16)
-    sq_tx[1:2, :] = to_row(att_sq)
-
-    def sq_copy(d):
-        return remote(
-            sq_tx, sq_rx.at[d], sq_s.at[d], sq_r.at[d], tp=lax.rem(tp + d, n_tp)
-        )
-
-    for d in range(1, n_tp):
-        sq_copy(d).start()
-    sums = sq_tx[...]
-    for d in range(1, n_tp):
-        sq_copy(d).wait_recv()
-        sums = sums + sq_rx[d]
-    scale = lax.rsqrt(sums * (1.0 / (channels * n_tp)) + EPS)
-    inv_r[...] = to_column(scale[0:1, :])
-    scale = lax.rsqrt(sums * (1.0 / (heads * VDIM * n_tp)) + EPS)
-    inv_a[...] = to_column(scale[1:2, :])
+    share_squares(1, att_sq)
+    join_squares(1, heads * VDIM * n_tp)
 
     def d2d_copy(dy, c):
         return remote(
@@ -429,22 +572,20 @@
         to = 2 * lax.rem(yy + dy, n_y) + core
         return remote(y_tx.at[dy, c], y_rx.at[dy, c], y_s.at[dy, c], y_r.at[dy, c], tp=to)
 
+    @jax.named_scope("produce")
     def produce(dy, c):
-        first = pl.multiple_of(2 * rd * lax.rem(yy + dy, n_y), 2 * rd)
-        at = pl.ds(first, 2 * rd)
-        cols = pl.ds(pl.multiple_of(c * cb, cb), cb)
-        pr[...] = dot(rb[at, :], wor[:, cols]) * inv_r[at, :] + dot(
-            ab[at, :], woa[:, cols]
-        ) * inv_a[at, :]
+        multiply(dy, c, ab, woa, True)
         theirs = pl.ds(pl.multiple_of((1 - core) * rd, rd), rd)
-        mine = pl.ds(pl.multiple_of(core * rd, rd), rd)
-        d2d_tx[dy, c] = pr[theirs, :].astype(BF16)
+        d2d_tx[dy, c] = prod[dy, c, theirs, :].astype(BF16)
         d2d_copy(dy, c).start()
-        comb[dy, c] = pr[mine, :]
-
+
+    def mine(dy, c):
+        return prod[dy, c, pl.ds(pl.multiple_of(core * rd, rd), rd), :]
+
+    @jax.named_scope("pair")
     def send_pair(dy, c):
         d2d_copy(dy, c).wait_recv()
-        y_tx[dy, c] = (comb[dy, c] + d2d_rx[dy, c].astype(F32)).astype(BF16)
+        y_tx[dy, c] = (mine(dy, c) + d2d_rx[dy, c].astype(F32)).astype(BF16)
         y_copy(dy, c).start()
 
     for dy in range(1, n_y):
@@ -467,9 +608,10 @@
 
     lax.fori_loop(0, COLS, home, 0)
 
+    @jax.named_scope("gather")
     def gather(c, total):
         d2d_copy(0, c).wait_recv()
-        value = comb[0, c] + d2d_rx[0, c].astype(F32)
+        value = mine(0, c) + d2d_rx[0, c].astype(F32)
         for dy in range(1, n_y):
             y_copy(dy, c).wait_recv()
             value = value + y_rx[dy, c].astype(F32)
@@ -483,6 +625,7 @@
         at = slice(c * cb, (c + 1) * cb)
         out_ref[:, at] = (mixed[c] * last * pgain[:, at]).astype(BF16)
 
+    @jax.named_scope("drain")
     def drain(r, _):
         for dy in range(1, n_y):
             tok_copy(dy, r).wait_send()
@@ -521,8 +664,9 @@
         return 0
 
     lax.fori_loop(1, n_sp - me, carry_done, 0)
-    for d in range(1, n_tp):
-        sq_copy(d).wait_send()
+    for kind in range(2):
+        for d in range(1, n_tp):
+            sq_copy(kind, d).wait_send()
 
     def sums_done(c, _):
         for dy in range(n_y):
@@ -552,21 +696,21 @@
     rd = rows // n_tp
     cb = width // COLS
 
-    lane = jnp.arange(LANES)
-    frequency = 1.0 / THETA ** ((2 * (lane % (ROPE // 2))).astype(F32) / ROPE)
-    places = (lax.axis_index("sp") * rows + jnp.arange(rows)).astype(F32)
-    turned = places[:, None] * frequency[None, :]
-    cosine = jnp.where(lane < ROPE, jnp.cos(turned), 0.0)
-    sine = jnp.sin(turned) * jnp.where(lane < ROPE // 2, -1.0, jnp.where(lane < ROPE, 1.0, 0.0))
+    lane = np.arange(LANES)
+    frequency = np.where(lane < ROPE, THETA ** (-2.0 * (lane % (ROPE // 2)) / ROPE), 0.0)
+    within = np.arange(rows)[:, None] * frequency
+    start = rows * np.arange(n_sp)[:, None, None] * frequency
+    turns = np.stack([np.cos(within), np.sin(within)]).astype(np.float32)
+    starts = np.stack([np.cos(start), np.sin(start)]).astype(np.float32)
 
     def row(v):
         return v.reshape(1, -1)
 
     args = (
         tokens, pre_gain.reshape(n_tp, 1, feats), row(rate_factor), w_rec_in, w_rec_gate,
-        conv_taps, rate_maps, input_maps, row(decay_param), w_query, w_latent, w_rope_key,
+        conv_taps, rate_maps, input_maps, row(decay_param), w_query, w_latent, w_rope_key.T,
         row(latent_gain), w_expand, row(rec_gain), row(att_gain), w_out_rec, w_out_att,
-        row(post_gain), cosine, sine,
+        row(post_gain), jnp.asarray(turns), jnp.asarray(starts),
     )
     vm = pltpu.VMEM
     dma = pltpu.SemaphoreType.DMA
@@ -581,23 +725,23 @@
         like(args[14]), like(args[15]), like(args[16]), like(args[17]), like(args[18]),
         like(args[19]), like(args[20]),
         vm((rows, latent), F32), vm((rows, LANES), F32), vm((rows, channels), F32),
-        vm((rows, channels), F32), vm((rows, q_pad), F32), vm((rows, 1), F32),
+        vm((rows, channels), F32), vm((rows, q_pad), F32), vm((rows, LANES), F32),
         vm((n_sp, rows, latent + LANES), BF16), vm((heads, rows, NOPE + LANES), BF16),
         vm((rows + 8, channels), F32), vm((rows, channels), F32),
-        vm((heads, rows, 1), F32), vm((heads, rows, 1), F32), vm((heads, rows, VDIM), F32),
+        vm((heads, rows, LANES), F32), vm((heads, rows, LANES), F32), vm((heads, rows, VDIM), F32),
         vm((rows, channels), F32), vm((rows, channels), F32),
         vm((rows, channels), BF16), vm((rows, heads * VDIM), BF16),
         vm((8, channels), F32), vm((8, channels), F32), vm((8, channels), F32),
-        vm((n_sp, 8, channels), F32), vm((8, rows), F32), vm((n_tp, 8, rows), F32),
-        vm((rows, 1), F32), vm((rows, 1), F32),
-        vm((2 * rd, cb), F32), vm((n_y, COLS, rd, cb), F32), vm((n_y, COLS, rd, cb), BF16),
+        vm((n_sp, 8, channels), F32), vm((2, 8, rows), F32), vm((2, n_tp, 8, rows), F32),
+        vm((2, rows, LANES), F32),
+        vm((n_y, COLS, 2 * rd, cb), F32), vm((n_y, COLS, rd, cb), BF16),
         vm((n_y, COLS, rd, cb), BF16), vm((n_y, COLS, rd, cb), BF16),
         vm((n_y, COLS, rd, cb), BF16), vm((COLS, rd, cb), F32),
-        dma((len(args),)), dma, dma, dma((n_y, CHUNKS)), dma((n_y, CHUNKS)),
+        dma((len(args),)), dma((5, n_tp)), dma, dma, dma((n_y, CHUNKS)), dma((n_y, CHUNKS)),
         dma((n_y, CHUNKS)), dma((n_y, CHUNKS)),
         dma((n_sp // 2, CHUNKS)), dma((n_sp, CHUNKS)), dma((n_sp, CHUNKS)),
         dma((n_sp, CHUNKS)), dma((n_sp, CHUNKS)),
-        dma((2,)), dma((n_sp,)), dma((n_sp,)), dma((n_tp,)), dma((n_tp,)),
+        dma((2,)), dma((n_sp,)), dma((n_sp,)), dma((2, n_tp)), dma((2, n_tp)),
         dma((n_y, COLS)), dma((n_y, COLS)), dma((n_y, COLS)), dma((n_y, COLS)),
     ]
     return pl.pallas_call(

time: 80.3 us -> 61.6 us (0.77)
  the two profiles are of different devices: /device:TPU:30 before, /device:TPU:24 now
where the time goes in v2:
time: 61.6 us; the launch traced here: 61.4 us
  Pallas kernels  59.6 us (97%)
  local copies, waits for them, and re-layouts  1.87 us (3%)
    pallas_call x1, Pallas kernels, shards(): pl.pallas_call(functools.partial(fused_kernel, n_sp, n_tp, heads), out_sh...  59.6 us
    unnamed x1, local copies, waits for them, and re-layouts  1.87 us

profile of v2, /device:TPU:24, one launch (start us, length us, event | category | flops | bytes accessed | tf_op | source)
XLA Modules:
  0.0 61.4 jit_solution(1086305854878683176)
XLA Ops:
  0.0 59.6 %layer.1 = bf16[64,4096]{1,0:T(8,128)(2,1)} custom-call(bf16[256,1024]{1,0:T(8,128)(2,1)} %tokens.1, f32[4,1,1024]{2,1,0:T(1,128)} %bitcast.9, f32[1,256]{1,0:T(1,128)} %bitcast.12, bf16[4096,256]{1,0:T(8,128)(2,1)} %w_rec.1, bf16[4096,256]{1,0:T(8,128)(2,1)} %w_gate.1, f32[4,256]{1,0:T(4,128)} %taps_in.1, bf16[2,128,128]{2,1,0:T(8,128)(2,1)} %rmap_in.1, ...), custom_call_target="tpu_custom_call" | custom-call | tf_op jit(solution)/shard_map/layer/pallas_call | solution.py:747
  59.6 1.9 %copy.23 = bf16[64,4096]{1,0:T(8,128)(2,1)} copy(bf16[64,4096]{1,0:T(8,128)(2,1)} %layer.1) | data formatting | bytes 1048576

commit v3 on v2

--- a/solution.py
+++ b/solution.py
@@ -18,7 +18,7 @@
 RATE_C = 8.0
 THETA = 10000.0
 CHUNKS = 4
-BATCH = 4
+BATCH = 8
 COLS = 4
 
 MESH = pl.DeviceIdType.MESH
@@ -63,14 +63,14 @@
     w_latent, w_rope, lat_gain_in, w_expand, rec_gain_in, att_gain_in, w_or, w_oa, post_gain_in,
     turns_in, starts_in,
     out_ref,
-    tok, scaled, gain, rate, wrec, wgate, taps, rmap, imap, decay, wq, wlat, wrope, lgain, wexp,
+    tok, scaled, gain, rate, wcat, taps, rmap, imap, decay, wrope, lgain, wexp,
     rgain, again, wor, woa, pgain, turns, starts,
     acc_lat, acc_rope, acc_rec, acc_gate, acc_q, sq, kv, qcat, padded, gated,
     m_ref, l_ref, o_ref, a_ref, b_ref, rb, ab,
     tail_tx, tail_rx, carry_tx, carry_rx, sq_tx, sq_rx, inv,
-    prod, d2d_tx, d2d_rx, y_tx, y_rx, mixed,
-    load_sem, weight_sem, own_tx, own_rx, tok_tx, tok_rx, fwd_tx, fwd_rx,
-    kvz_tx, kvx_tx, kv_rx, kvd_tx, kvd_rx,
+    prod, held, own, d2d_tx, d2d_rx, y_tx, y_rx, mixed, done, out_sem,
+    load_sem, weight_sem, own_sem, tok_tx, tok_rx, fwd_tx, fwd_rx,
+    kvz_tx, kvx_tx, kvd_tx, kvz_rx, kvx_rx, kvd_rx,
     tail_s, carry_s, carry_r, sq_s, sq_r, d2d_s, d2d_r, y_s, y_r,
 ):
     me = lax.axis_index("sp")
@@ -101,7 +101,10 @@
         (decay_in, decay), (rec_gain_in, rgain), (att_gain_in, again), (w_or, wor), (w_oa, woa),
         (post_gain_in, pgain),
     )
-    projections = ((w_latent, wlat), (w_rec, wrec), (w_gate, wgate), (w_query, wq))
+    projections = []
+    for s in (w_latent, w_rec, w_gate, w_query):
+        first = projections[-1][2] if projections else 0
+        projections.append((s, first, first + s.shape[1]))
 
     def loads_of(group, first):
         return [
@@ -114,9 +117,16 @@
     def weight_loads(blk):
         at = features(blk)
         copies = [pltpu.make_async_copy(w_rope.at[:, at], wrope.at[:, at], weight_sem.at[0, blk])]
-        for i, (s, d) in enumerate(projections):
-            copies.append(pltpu.make_async_copy(s.at[at], d.at[at], weight_sem.at[1 + i, blk]))
+        for s, first, last in projections:
+            copies.append(
+                pltpu.make_async_copy(s.at[at], wcat.at[at, first:last], weight_sem.at[1, blk])
+            )
         return copies
+
+    def weights_ready(blk):
+        at = features(blk)
+        weight_loads(blk)[0].wait()
+        pltpu.make_async_copy(wcat.at[at], wcat.at[at], weight_sem.at[1, blk]).wait()
 
     first_loads = loads_of(small, 0)
     last_loads = loads_of(later, len(small))
@@ -161,16 +171,16 @@
         return pl.ds(pl.multiple_of(r * rc + core * hc, hc), hc)
 
     def own_copy():
-        return remote(tok.at[tp], tok.at[tp], own_tx, own_rx, tp=partner)
+        return remote(tok.at[tp], tok.at[tp], own_sem.at[0], own_sem.at[1], tp=partner)
 
     def tok_copy(dy, r):
         to = 2 * lax.rem(yy + dy, n_y) + core
         part = tok.at[tp, chunk(r)]
-        return remote(part, part, tok_tx.at[dy, r], tok_rx.at[dy, r], tp=to)
+        return remote(part, part, tok_tx, tok_rx.at[dy - 1, r], tp=to)
 
     def fwd_copy(dy, r):
         part = tok.at[2 * lax.rem(yy + n_y - dy, n_y) + core, chunk(r)]
-        return remote(part, part, fwd_tx.at[dy, r], fwd_rx.at[dy, r], tp=partner)
+        return remote(part, part, fwd_tx, fwd_rx.at[dy - 1, r], tp=partner)
 
     for step in range(CHUNKS):
         for dy in range(1, n_y):
@@ -207,14 +217,14 @@
         k = features(blk)
         x = scaled[at, :]
         acc_rope[at, : wrope.shape[0]] += dot_t(x, wrope[:, k])
-        acc_lat[at, :] += dot(x, wlat[k, :])
+        acc_lat[at, :] += dot(x, wcat[k, :latent])
 
     @jax.named_scope("late")
     def project_late(blk, at):
         k = features(blk)
         x = scaled[at, :]
-        for w, acc in ((wrec, acc_rec), (wgate, acc_gate), (wq, acc_q)):
-            acc[at, : w.shape[1]] += dot(x, w[k, :])
+        for (_, first, last), acc in zip(projections[1:], (acc_rec, acc_gate, acc_q)):
+            acc[at, : last - first] += dot(x, wcat[k, first:last])
 
     for copy in first_loads[1:]:
         copy.wait()
@@ -225,12 +235,11 @@
 
         @pl.when(i == 1)
         def _():
-            own_copy().wait()
+            own_copy().wait_recv()
 
         scale_rows(blk, 0, rows)
         with jax.named_scope("weights"):
-            for copy in weight_loads(blk):
-                copy.wait()
+            weights_ready(blk)
         project_early(blk, everything)
         project_late(blk, everything)
         return 0
@@ -239,23 +248,40 @@
     for copy in last_loads:
         copy.start()
 
-    def kvz_copy(dz, r):
-        part = kv.at[me, half(r)]
-        return remote(part, part, kvz_tx.at[dz, r], kv_rx.at[me, r], sp=me + 2 * dz)
+    def settle(count, most, wait):
+        for k in range(1, most + 1):
+            @pl.when(count == k)
+            def _():
+                wait(k)
+
+    def upwards(s, r):
+        part = kv.at[s, half(r)]
+        for dz in range(1, min(3, levels)):
+            @pl.when(level + dz < levels)
+            def _():
+                (
+                    remote(part, part, kvz_tx, kvz_rx.at[level + dz - lax.div(s, 2), r], sp=me + 2 * dz)
+                ).start()
 
     def kvx_copy(s, r):
         part = kv.at[s, half(r)]
-        return remote(part, part, kvx_tx.at[s, r], kv_rx.at[s, r], sp=neighbour)
+        return remote(part, part, kvx_tx, kvx_rx.at[r], sp=neighbour)
 
     def kvd_copy(s, r):
         part = kv.at[s, half(r)]
-        return remote(part, part, kvd_tx.at[s, r], kvd_rx.at[s, r], tp=partner)
+        return remote(part, part, kvd_tx, kvd_rx.at[r], tp=partner)
 
     @jax.named_scope("fwdz")
     def forward_z(r, near, far):
         def body(dz, _):
             s = me - 2 * dz
-            kvx_copy(s, r).wait_recv()
+            part = kv.at[s, half(r)]
+            remote(part, part, kvz_tx, kvz_rx.at[dz, r], sp=neighbour).wait_recv()
+
+            @pl.when(lax.rem(dz, 2) == 0)
+            def _():
+                upwards(s, r)
+
             kvx_copy(s, r).start()
             kvd_copy(s, r).start()
             return 0
@@ -265,10 +291,14 @@
     @jax.named_scope("fwdx")
     def forward_x(r):
         def body(dz, _):
-            s = neighbour - 2 * dz
-            kvx_copy(s, r).wait_recv()
-            kvd_copy(s, r).start()
+            kvd_copy(neighbour - 2 * dz, r).start()
             return 0
+
+        def arrived(k):
+            part = kv.at[0:k, 0:hc]
+            remote(part, part, kvx_tx, kvx_rx.at[r], sp=neighbour).wait_recv()
+
+        settle(level + column, levels, arrived)
 
         lax.fori_loop(1 - column, level + 1, body, 0)
 
@@ -292,10 +322,7 @@
         norm = raw * lax.rsqrt(jnp.mean(raw * raw, axis=1, keepdims=True) + EPS) * lgain[...]
         kv[me, at, :latent] = norm.astype(BF16)
         kv[me, at, latent:] = rotate(acc_rope[at, :] * inverse, cosine, sine).astype(BF16)
-        for dz in range(1, levels):
-            @pl.when(level + dz < levels)
-            def _():
-                kvz_copy(dz, r).start()
+        upwards(me, r)
 
         @pl.when(column == 0)
         def _():
@@ -315,12 +342,20 @@
                 if b == 1:
                     with jax.named_scope("fwdwait"):
                         fwd_copy(dy, r).wait_recv()
+                    if dy == 1:
+                        @pl.when(step > 1)
+                        def _():
+                            forward_z(r + 2, 2, 3)
+
+                        @pl.when(step > 2)
+                        def _():
+                            forward_z(r + 3, 3, levels)
+
                 scale_rows(blk, r * rc, rc)
 
                 @pl.when(step == 0)
                 def _():
-                    for copy in weight_loads(blk):
-                        copy.wait()
+                    weights_ready(blk)
 
                 project_early(blk, at)
                 if b == 1 and dy == n_y - 1:
@@ -353,16 +388,14 @@
         def _():
             forward_z(r + 1, 1, 2)
 
-        @pl.when(step > 1)
-        def _():
-            forward_z(r + 2, 2, levels)
-
         return 0
 
     def tail_copy():
         return remote(tail_tx, tail_rx, tail_s.at[0], tail_s.at[1], sp=me + 1)
 
     lax.fori_loop(0, CHUNKS, tok_step, 0)
+
+    forward_z(1, 2, 3)
 
     for copy in last_loads:
         copy.wait()
@@ -421,7 +454,7 @@
 
     def carry_copy(d):
         return remote(
-            carry_tx, carry_rx.at[me], carry_s.at[d], carry_r.at[me], sp=me + d
+            carry_tx, carry_rx.at[me], carry_s, carry_r, sp=me + d
         )
 
     def carry_start(d, _):
@@ -429,9 +462,7 @@
         return 0
 
     lax.fori_loop(1, n_sp - me, carry_start, 0)
-
-    forward_z(0, 1, 2)
-    forward_z(1, 2, levels)
+    forward_z(2, 3, levels)
 
     root = 1.0 / math.sqrt(NOPE + ROPE)
 
@@ -465,12 +496,12 @@
             o_ref[h] = found
 
     def attend_chunk(r):
-        def ready(s, _):
-            kvd_copy(s, r).wait_recv()
-            return 0
+        def ready(k):
+            part = kv.at[0:k, 0:hc]
+            remote(part, part, kvd_tx, kvd_rx.at[r], tp=partner).wait_recv()
 
         with jax.named_scope("kvwait"):
-            lax.fori_loop(0, me, ready, 0)
+            settle(me, n_sp - 1, ready)
 
         def group(g, _):
             several = pl.ds(g * BATCH, BATCH)
@@ -485,12 +516,13 @@
         lax.fori_loop(0, lax.div(me + BATCH - 1, BATCH), group, 0)
 
     attend(kv[me, :, :latent], kv[me, :, latent:], None)
-    forward_z(0, 2, levels)
+    forward_z(0, 1, 2)
+    forward_z(0, 2, 3)
+    forward_z(1, 3, levels)
 
     def sq_copy(kind, d):
         return remote(
-            sq_tx.at[kind], sq_rx.at[kind, d], sq_s.at[kind, d], sq_r.at[kind, d],
-            tp=lax.rem(tp + d, n_tp),
+            sq_tx.at[kind], sq_rx.at[kind, d], sq_s, sq_r.at[kind], tp=lax.rem(tp + d, n_tp)
         )
 
     def share_squares(kind, column):
@@ -501,8 +533,9 @@
     @jax.named_scope("sums")
     def join_squares(kind, count):
         total = sq_tx[kind]
+        part = sq_rx.at[kind, 1:n_tp]
+        remote(part, part, sq_s, sq_r.at[kind], tp=partner).wait_recv()
         for d in range(1, n_tp):
-            sq_copy(kind, d).wait_recv()
             total = total + sq_rx[kind, d]
         scale = lax.rsqrt(total * (1.0 / count) + EPS)
         inv[kind] = jnp.broadcast_to(to_column(scale[0:1, :]), inv.shape[1:])
@@ -510,11 +543,13 @@
     @jax.named_scope("join")
     def finish_recurrence():
         def join(s, carried):
-            remote(
-                carry_tx, carry_rx.at[s], carry_s.at[0], carry_r.at[s], sp=neighbour
-            ).wait_recv()
             return carry_rx[s, 0:1, :] * carried + carry_rx[s, 1:2, :]
 
+        def arrived(k):
+            part = carry_rx.at[0:k]
+            remote(part, part, carry_s, carry_r, sp=neighbour).wait_recv()
+
+        settle(me, n_sp - 1, arrived)
         carried = lax.fori_loop(0, me, join, jnp.zeros((1, channels), F32))
         rec_out = (b_ref[...] + a_ref[...] * carried) * gated[...]
         rb[...] = (rec_out * rgain[...]).astype(BF16)
@@ -526,32 +561,71 @@
     def cols(c):
         return pl.ds(pl.multiple_of(c * cb, cb), cb)
 
-    @jax.named_scope("recprod")
-    def multiply(dy, c, left, right, add):
-        at = block(dy)
-        value = dot(left[at, :], right[:, cols(c)])
-        if add:
-            count = cb // LANES
-            value = value * wide(inv[1, at, :], count) + prod[dy, c] * wide(inv[0, at, :], count)
-        prod[dy, c] = value
-
-    forward_x(CHUNKS - 1)
-    forward_x(CHUNKS - 2)
-    attend_chunk(CHUNKS - 1)
-    for r in range(CHUNKS - 3, 0, -1):
-        forward_x(r)
-        attend_chunk(r + 1)
+    @jax.named_scope("multiply")
+    def multiply(dy, c, left, right, store):
+        store[dy, c] = dot(left[block(dy), :], right[:, cols(c)])
+
+    def d2d_copy(dy, c):
+        return remote(
+            d2d_tx.at[dy, c], d2d_rx.at[dy, c], d2d_s, d2d_r.at[dy, c], tp=partner
+        )
+
+    def y_copy(dy, c):
+        to = 2 * lax.rem(yy + dy, n_y) + core
+        return remote(y_tx.at[dy, c], y_rx.at[dy, c], y_s, y_r.at[dy - 1, c], tp=to)
+
+    def hand_over(dy, c, value):
+        held[...] = value
+        theirs = pl.ds(pl.multiple_of((1 - core) * rd, rd), rd)
+        mine = pl.ds(pl.multiple_of(core * rd, rd), rd)
+        d2d_tx[dy, c] = held[theirs, :].astype(BF16)
+        d2d_copy(dy, c).start()
+        own[dy, c] = held[mine, :]
+
+    def product(dy, c, left, right):
+        return dot(left[block(dy), :], right[:, cols(c)])
+
+    @jax.named_scope("produce")
+    def produce(dy, c):
+        at, count = block(dy), cb // LANES
+        hand_over(
+            dy, c,
+            prod[dy, c] * wide(inv[0, at, :], count)
+            + product(dy, c, ab, woa) * wide(inv[1, at, :], count),
+        )
+
+    @jax.named_scope("pair")
+    def send_pair(dy, c):
+        d2d_copy(dy, c).wait_recv()
+        y_tx[dy, c] = (own[dy, c] + d2d_rx[dy, c].astype(F32)).astype(BF16)
+        y_copy(dy, c).start()
+
+    @jax.named_scope("multiply")
+    def rec_products(dy):
+        def body(c, _):
+            prod[dy, c] = product(dy, c, rb, wor)
+            return 0
+
+        lax.fori_loop(1, COLS, body, 0)
+
+    forward_x(3)
     finish_recurrence()
+    for dy in range(1, n_y):
+        hand_over(dy, COLS, product(dy, 0, rb, wor))
+    forward_z(0, 3, levels)
+    attend_chunk(3)
+    for dy in range(1, n_y):
+        send_pair(dy, COLS)
+    forward_x(2)
+    for dy in range(1, n_y):
+        rec_products(dy)
+    attend_chunk(2)
+    forward_x(1)
+    hand_over(0, COLS, product(0, 0, rb, wor))
+    rec_products(0)
+    join_squares(0, channels * n_tp)
     attend_chunk(1)
     forward_x(0)
-
-    for dy in range(n_y):
-        def rec_product(c, _):
-            multiply(dy, c, rb, wor, False)
-            return 0
-
-        lax.fori_loop(0, COLS, rec_product, 0)
-    join_squares(0, channels * n_tp)
     attend_chunk(0)
 
     att_sq = jnp.zeros((rows, 1), F32)
@@ -561,32 +635,11 @@
         at = slice(h * VDIM, (h + 1) * VDIM)
         ab[:, at] = (att * again[:, at]).astype(BF16)
     share_squares(1, att_sq)
+    for dy in range(1, n_y):
+        hand_over(dy, 0, product(dy, 0, ab, woa))
+    for dy in range(1, n_y):
+        send_pair(dy, 0)
     join_squares(1, heads * VDIM * n_tp)
-
-    def d2d_copy(dy, c):
-        return remote(
-            d2d_tx.at[dy, c], d2d_rx.at[dy, c], d2d_s.at[dy, c], d2d_r.at[dy, c], tp=partner
-        )
-
-    def y_copy(dy, c):
-        to = 2 * lax.rem(yy + dy, n_y) + core
-        return remote(y_tx.at[dy, c], y_rx.at[dy, c], y_s.at[dy, c], y_r.at[dy, c], tp=to)
-
-    @jax.named_scope("produce")
-    def produce(dy, c):
-        multiply(dy, c, ab, woa, True)
-        theirs = pl.ds(pl.multiple_of((1 - core) * rd, rd), rd)
-        d2d_tx[dy, c] = prod[dy, c, theirs, :].astype(BF16)
-        d2d_copy(dy, c).start()
-
-    def mine(dy, c):
-        return prod[dy, c, pl.ds(pl.multiple_of(core * rd, rd), rd), :]
-
-    @jax.named_scope("pair")
-    def send_pair(dy, c):
-        d2d_copy(dy, c).wait_recv()
-        y_tx[dy, c] = (mine(dy, c) + d2d_rx[dy, c].astype(F32)).astype(BF16)
-        y_copy(dy, c).start()
 
     for dy in range(1, n_y):
         def away(c, _):
@@ -594,88 +647,92 @@
             def _():
                 produce(dy, c)
 
-            @pl.when(c > 0)
+            @pl.when(c > 1)
             def _():
                 send_pair(dy, c - 1)
 
             return 0
 
-        lax.fori_loop(0, COLS + 1, away, 0)
+        lax.fori_loop(1, COLS + 1, away, 0)
+
+    hand_over(0, 0, product(0, 0, ab, woa))
 
     def home(c, _):
         produce(0, c)
         return 0
 
-    lax.fori_loop(0, COLS, home, 0)
-
-    @jax.named_scope("gather")
-    def gather(c, total):
+    lax.fori_loop(1, COLS, home, 0)
+
+    def gone(part, sem):
+        remote(part, part, sem, own_sem.at[1], tp=partner).wait_send()
+
+    with jax.named_scope("drain"):
+        gone(tok.at[tp], own_sem.at[0])
+        gone(tok.at[0 : n_y - 1], tok_tx)
+        gone(tok.at[0 : n_y - 1], fwd_tx)
+        for at in range(levels - 1):
+            @pl.when(level == at)
+            def _():
+                count = (1 + at // 2) * min(2, levels - 1 - at)
+                gone(kv.at[0:count, 0 : CHUNKS * hc], kvz_tx)
+
+        settle(level + 1 - column, levels, lambda k: gone(kv.at[0:k, 0 : CHUNKS * hc], kvx_tx))
+        settle(me, n_sp - 1, lambda k: gone(kv.at[0:k, 0 : CHUNKS * hc], kvd_tx))
+        settle(n_sp - 1 - me, n_sp - 1, lambda k: gone(carry_rx.at[0:k], carry_s))
+        gone(sq_rx.at[:, 1:n_tp], sq_s)
+
+        @pl.when(me + 1 < n_sp)
+        def _():
+            tail_copy().wait_send()
+
+    my_rows = pl.ds(pl.multiple_of(tp * rd, rd), rd)
+
+    def summed(c):
         d2d_copy(0, c).wait_recv()
-        value = mine(0, c) + d2d_rx[0, c].astype(F32)
+        value = own[0, c] + d2d_rx[0, c].astype(F32)
         for dy in range(1, n_y):
             y_copy(dy, c).wait_recv()
             value = value + y_rx[dy, c].astype(F32)
+        return value
+
+    @jax.named_scope("gather")
+    def first_columns():
+        count = cb // LANES
+        value = summed(COLS) * wide(inv[0, my_rows, :], count)
+        value = value + summed(0) * wide(inv[1, my_rows, :], count)
+        mixed[0] = value
+        return jnp.sum(value * value, axis=1, keepdims=True)
+
+    @jax.named_scope("gather")
+    def gather(c, total):
+        value = summed(c)
         mixed[c] = value
         return total + jnp.sum(value * value, axis=1, keepdims=True)
 
-    total = lax.fori_loop(0, COLS, gather, jnp.zeros((rd, 1), F32))
+    total = lax.fori_loop(1, COLS, gather, first_columns())
+
+    def out_copy(at):
+        return pltpu.make_async_copy(done.at[:, at], out_ref.at[:, at], out_sem)
+
+    mark = jax.named_scope("final")
+    mark.__enter__()
     last = lax.rsqrt(total * (1.0 / width) + EPS)
 
     for c in range(COLS):
         at = slice(c * cb, (c + 1) * cb)
-        out_ref[:, at] = (mixed[c] * last * pgain[:, at]).astype(BF16)
-
-    @jax.named_scope("drain")
-    def drain(r, _):
-        for dy in range(1, n_y):
-            tok_copy(dy, r).wait_send()
-            fwd_copy(dy, r).wait_send()
-        for dz in range(1, levels):
-            @pl.when(level + dz < levels)
-            def _():
-                kvz_copy(dz, r).wait_send()
-
-        @pl.when(column == 0)
-        def _():
-            kvx_copy(me, r).wait_send()
-
-        def sent_z(dz, _):
-            kvx_copy(me - 2 * dz, r).wait_send()
-            kvd_copy(me - 2 * dz, r).wait_send()
-            return 0
-
-        lax.fori_loop(1, level + 1, sent_z, 0)
-
-        def sent_x(dz, _):
-            kvd_copy(neighbour - 2 * dz, r).wait_send()
-            return 0
-
-        lax.fori_loop(1 - column, level + 1, sent_x, 0)
-        return 0
-
-    lax.fori_loop(0, CHUNKS, drain, 0)
-
-    @pl.when(me + 1 < n_sp)
-    def _():
-        tail_copy().wait_send()
-
-    def carry_done(d, _):
-        carry_copy(d).wait_send()
-        return 0
-
-    lax.fori_loop(1, n_sp - me, carry_done, 0)
-    for kind in range(2):
-        for d in range(1, n_tp):
-            sq_copy(kind, d).wait_send()
-
-    def sums_done(c, _):
-        for dy in range(n_y):
-            d2d_copy(dy, c).wait_send()
-            if dy > 0:
-                y_copy(dy, c).wait_send()
-        return 0
-
-    lax.fori_loop(0, COLS, sums_done, 0)
+        done[:, at] = (mixed[c] * last * pgain[:, at]).astype(BF16)
+        out_copy(at).start()
+
+    mark.__exit__(None, None, None)
+    with jax.named_scope("outwait"):
+        out_copy(slice(0, width)).wait()
+
+    mark = jax.named_scope("sumsdone")
+    mark.__enter__()
+
+    gone(d2d_tx, d2d_s)
+    gone(y_tx.at[1:n_y], y_s)
+    mark.__exit__(None, None, None)
 
 
 def shards(
@@ -720,8 +777,9 @@
 
     scratch = [
         vm((n_tp, rows, feats), BF16), vm((rows, feats), BF16), like(args[1]), like(args[2]),
-        like(args[3]), like(args[4]), like(args[5]), like(args[6]), like(args[7]), like(args[8]),
-        like(args[9]), like(args[10]), like(args[11]), like(args[12]), like(args[13]),
+        vm((width, latent + 2 * channels + q_cols), BF16),
+        like(args[5]), like(args[6]), like(args[7]), like(args[8]),
+        like(args[11]), like(args[12]), like(args[13]),
         like(args[14]), like(args[15]), like(args[16]), like(args[17]), like(args[18]),
         like(args[19]), like(args[20]),
         vm((rows, latent), F32), vm((rows, LANES), F32), vm((rows, channels), F32),
@@ -734,21 +792,22 @@
         vm((8, channels), F32), vm((8, channels), F32), vm((8, channels), F32),
         vm((n_sp, 8, channels), F32), vm((2, 8, rows), F32), vm((2, n_tp, 8, rows), F32),
         vm((2, rows, LANES), F32),
-        vm((n_y, COLS, 2 * rd, cb), F32), vm((n_y, COLS, rd, cb), BF16),
-        vm((n_y, COLS, rd, cb), BF16), vm((n_y, COLS, rd, cb), BF16),
-        vm((n_y, COLS, rd, cb), BF16), vm((COLS, rd, cb), F32),
-        dma((len(args),)), dma((5, n_tp)), dma, dma, dma((n_y, CHUNKS)), dma((n_y, CHUNKS)),
-        dma((n_y, CHUNKS)), dma((n_y, CHUNKS)),
-        dma((n_sp // 2, CHUNKS)), dma((n_sp, CHUNKS)), dma((n_sp, CHUNKS)),
-        dma((n_sp, CHUNKS)), dma((n_sp, CHUNKS)),
-        dma((2,)), dma((n_sp,)), dma((n_sp,)), dma((2, n_tp)), dma((2, n_tp)),
-        dma((n_y, COLS)), dma((n_y, COLS)), dma((n_y, COLS)), dma((n_y, COLS)),
+        vm((n_y, COLS, 2 * rd, cb), F32), vm((2 * rd, cb), F32),
+        vm((n_y, COLS + 1, rd, cb), F32), vm((n_y, COLS + 1, rd, cb), BF16),
+        vm((n_y, COLS + 1, rd, cb), BF16), vm((n_y, COLS + 1, rd, cb), BF16),
+        vm((n_y, COLS + 1, rd, cb), BF16), vm((COLS, rd, cb), F32), vm((rd, width), BF16),
+        dma,
+        dma((16,)), dma((2, n_tp)), dma((2,)), dma, dma((n_y - 1, CHUNKS)),
+        dma, dma((n_y - 1, CHUNKS)),
+        dma, dma, dma, dma((n_sp // 2, CHUNKS)), dma((CHUNKS,)), dma((CHUNKS,)),
+        dma((2,)), dma, dma, dma, dma((2,)),
+        dma, dma((n_y, COLS + 1)), dma, dma((n_y - 1, COLS + 1)),
     ]
     return pl.pallas_call(
         functools.partial(fused_kernel, n_sp, n_tp, heads),
         out_shape=jax.ShapeDtypeStruct((rd, width), BF16),
         in_specs=[pl.BlockSpec(memory_space=pl.ANY)] * len(args),
-        out_specs=pl.BlockSpec(memory_space=pltpu.VMEM),
+        out_specs=pl.BlockSpec(memory_space=pl.ANY),
         scratch_shapes=scratch,
         compiler_params=pltpu.CompilerParams(
             collective_id=0, has_side_effects=True, vmem_limit_bytes=67043328

time: 61.6 us -> 53.6 us (0.87)
  Pallas kernels: 59.6 us -> 51.6 us
    pallas_call x1, Pallas kernels: 59.6 us -> 51.6 us  [shards(): pl.pallas_call(functools.partial(fused_kernel, n_sp, n_tp, heads), out_sh...]
where the time goes in v3:
time: 53.6 us; the launch traced here: 53.5 us
  Pallas kernels  51.6 us (96%)
  local copies, waits for them, and re-layouts  1.87 us (3%)
    pallas_call x1, Pallas kernels, shards(): pl.pallas_call(functools.partial(fused_kernel, n_sp, n_tp, heads), out_sh...  51.6 us
    unnamed x1, local copies, waits for them, and re-layouts  1.87 us

profile of v3, /device:TPU:24, one launch (start us, length us, event | category | flops | bytes accessed | tf_op | source)
XLA Modules:
  0.0 53.5 jit_solution(9030953353579242)
XLA Ops:
  0.0 51.6 %layer.1 = bf16[64,4096]{1,0:T(8,128)(2,1)} custom-call(bf16[256,1024]{1,0:T(8,128)(2,1)} %tokens.1, f32[4,1,1024]{2,1,0:T(1,128)} %bitcast.9, f32[1,256]{1,0:T(1,128)} %bitcast.12, bf16[4096,256]{1,0:T(8,128)(2,1)} %w_rec.1, bf16[4096,256]{1,0:T(8,128)(2,1)} %w_gate.1, f32[4,256]{1,0:T(4,128)} %taps_in.1, bf16[2,128,128]{2,1,0:T(8,128)(2,1)} %rmap_in.1, ...), custom_call_target="tpu_custom_call" | custom-call | tf_op jit(solution)/shard_map/layer/pallas_call | solution.py:806
  51.6 1.9 %copy.23 = bf16[64,4096]{1,0:T(8,128)(2,1)} copy(bf16[64,4096]{1,0:T(8,128)(2,1)} %layer.1) | data formatting | bytes 1048576

commit v4 on v3

--- a/solution.py
+++ b/solution.py
@@ -19,6 +19,7 @@
 THETA = 10000.0
 CHUNKS = 4
 BATCH = 8
+SPLIT = 2
 COLS = 4
 
 MESH = pl.DeviceIdType.MESH
@@ -68,7 +69,7 @@
     acc_lat, acc_rope, acc_rec, acc_gate, acc_q, sq, kv, qcat, padded, gated,
     m_ref, l_ref, o_ref, a_ref, b_ref, rb, ab,
     tail_tx, tail_rx, carry_tx, carry_rx, sq_tx, sq_rx, inv,
-    prod, held, own, d2d_tx, d2d_rx, y_tx, y_rx, mixed, done, out_sem,
+    prod, held, own, d2d_tx, d2d_rx, y_tx, y_rx, mixed, done, out_sem, known,
     load_sem, weight_sem, own_sem, tok_tx, tok_rx, fwd_tx, fwd_rx,
     kvz_tx, kvx_tx, kvd_tx, kvz_rx, kvx_rx, kvd_rx,
     tail_s, carry_s, carry_r, sq_s, sq_r, d2d_s, d2d_r, y_s, y_r,
@@ -114,34 +115,47 @@
     def features(blk):
         return pl.ds(pl.multiple_of(blk * feats, feats), feats)
 
+    def rope_load(blk):
+        at = features(blk)
+        return pltpu.make_async_copy(w_rope.at[:, at], wrope.at[:, at], weight_sem.at[0, blk])
+
     def weight_loads(blk):
         at = features(blk)
-        copies = [pltpu.make_async_copy(w_rope.at[:, at], wrope.at[:, at], weight_sem.at[0, blk])]
-        for s, first, last in projections:
-            copies.append(
-                pltpu.make_async_copy(s.at[at], wcat.at[at, first:last], weight_sem.at[1, blk])
-            )
-        return copies
+        return [rope_load(blk)] + [
+            pltpu.make_async_copy(s.at[at], wcat.at[at, first:last], weight_sem.at[1, blk])
+            for s, first, last in projections
+        ]
 
     def weights_ready(blk):
         at = features(blk)
-        weight_loads(blk)[0].wait()
+        rope_load(blk).wait()
         pltpu.make_async_copy(wcat.at[at], wcat.at[at], weight_sem.at[1, blk]).wait()
 
     first_loads = loads_of(small, 0)
     last_loads = loads_of(later, len(small))
     for copy in first_loads:
         copy.start()
-    for dy in range(n_y):
+
+    def start_weights(dy):
         for b in range(2):
             for copy in weight_loads(2 * lax.rem(yy + dy, n_y) + lax.rem(core + b, 2)):
                 copy.start()
 
     barrier = pltpu.get_barrier_semaphore()
-    for d in range(1, n_sp):
-        pl.semaphore_signal(
-            barrier, inc=1, device_id={"sp": lax.rem(me + d, n_sp)}, device_id_type=MESH
-        )
+    near = [o for step in (1, 2, 4) for o in (step, -step)]
+    inside = [(me + o >= 0) & (me + o < n_sp) for o in near]
+    near_count = functools.reduce(jnp.add, [x.astype(jnp.int32) for x in inside])
+
+    def tell_near(sem):
+        for o, x in zip(near, inside):
+            @pl.when(x)
+            def _():
+                pl.semaphore_signal(
+                    sem, inc=1, device_id={"sp": me + o}, device_id_type=MESH
+                )
+
+    rounds = known.shape[0]
+    tell_near(barrier)
     for d in range(1, n_tp):
         pl.semaphore_signal(
             barrier, inc=1, device_id={"tp": lax.rem(tp + d, n_tp)}, device_id_type=MESH
@@ -155,8 +169,10 @@
             return 0
 
         lax.fori_loop(me + 1, lax.div(me + BATCH - 1, BATCH) * BATCH, blank, 0)
-        pl.semaphore_wait(barrier, n_sp + n_tp - 2)
         first_loads[0].wait()
+        start_weights(0)
+        pl.semaphore_wait(barrier, near_count + n_tp - 1)
+        tell_near(known.at[0])
 
     def remote(src, dst, send, recv, **where):
         return pltpu.make_async_remote_copy(
@@ -186,6 +202,12 @@
         for dy in range(1, n_y):
             tok_copy(dy, CHUNKS - 1 - step).start()
     own_copy().start()
+
+    @jax.named_scope("tokwait")
+    def pass_on(r):
+        for dy in range(1, n_y):
+            tok_copy(dy, r).wait_recv()
+            fwd_copy(dy, r).start()
 
     def dot(a, b):
         return jnp.dot(a, b, preferred_element_type=F32)
@@ -240,6 +262,12 @@
         scale_rows(blk, 0, rows)
         with jax.named_scope("weights"):
             weights_ready(blk)
+
+        @pl.when(i == 0)
+        def _():
+            for dy in range(1, n_y):
+                start_weights(dy)
+
         project_early(blk, everything)
         project_late(blk, everything)
         return 0
@@ -247,6 +275,9 @@
     lax.fori_loop(0, 2, own_chip, 0)
     for copy in last_loads:
         copy.start()
+    for k in range(rounds - 1):
+        pl.semaphore_wait(known.at[k], near_count)
+        tell_near(known.at[k + 1])
 
     def settle(count, most, wait):
         for k in range(1, most + 1):
@@ -331,10 +362,7 @@
     def tok_step(step, _):
         r = CHUNKS - 1 - step
         at = chunk(r)
-        with jax.named_scope("tokwait"):
-            for dy in range(1, n_y):
-                tok_copy(dy, r).wait_recv()
-                fwd_copy(dy, r).start()
+        pass_on(r)
 
         for b in range(2):
             for dy in range(1, n_y):
@@ -461,8 +489,8 @@
         carry_copy(d).start()
         return 0
 
+    pl.semaphore_wait(known.at[rounds - 1], near_count)
     lax.fori_loop(1, n_sp - me, carry_start, 0)
-    forward_z(2, 3, levels)
 
     root = 1.0 / math.sqrt(NOPE + ROPE)
 
@@ -503,22 +531,26 @@
         with jax.named_scope("kvwait"):
             settle(me, n_sp - 1, ready)
 
-        def group(g, _):
-            several = pl.ds(g * BATCH, BATCH)
-            count = BATCH * rc
+        def several(first, blocks):
+            these = pl.ds(first, blocks)
+            count = blocks * rc
             attend(
-                kv[several, chunk(r), :latent].reshape(count, latent),
-                kv[several, chunk(r), latent:].reshape(count, LANES),
-                (me - g * BATCH) * rc,
+                kv[these, chunk(r), :latent].reshape(count, latent),
+                kv[these, chunk(r), latent:].reshape(count, LANES),
+                (me - first) * rc,
             )
-            return 0
-
-        lax.fori_loop(0, lax.div(me + BATCH - 1, BATCH), group, 0)
-
-    attend(kv[me, :, :latent], kv[me, :, latent:], None)
-    forward_z(0, 1, 2)
-    forward_z(0, 2, 3)
-    forward_z(1, 3, levels)
+
+        @pl.when((me > 0) & (me <= BATCH // 2))
+        def _():
+            several(0, BATCH // 2)
+
+        @pl.when(me > BATCH // 2)
+        def _():
+            def group(g, _):
+                several(g * BATCH, BATCH)
+                return 0
+
+            lax.fori_loop(0, lax.div(me + BATCH - 1, BATCH), group, 0)
 
     def sq_copy(kind, d):
         return remote(
@@ -606,26 +638,34 @@
             prod[dy, c] = product(dy, c, rb, wor)
             return 0
 
-        lax.fori_loop(1, COLS, body, 0)
-
+        lax.fori_loop(SPLIT, COLS, body, 0)
+
+    forward_z(2, 3, levels)
     forward_x(3)
+    attend(kv[me, :, :latent], kv[me, :, latent:], None)
+    forward_z(0, 1, 2)
+    attend_chunk(3)
+    forward_z(0, 2, 3)
+    forward_z(1, 3, levels)
+    forward_x(2)
     finish_recurrence()
     for dy in range(1, n_y):
-        hand_over(dy, COLS, product(dy, 0, rb, wor))
+        for c in range(SPLIT):
+            hand_over(dy, COLS + c, product(dy, c, rb, wor))
     forward_z(0, 3, levels)
-    attend_chunk(3)
+    attend_chunk(2)
     for dy in range(1, n_y):
-        send_pair(dy, COLS)
-    forward_x(2)
+        for c in range(SPLIT):
+            send_pair(dy, COLS + c)
+    forward_x(1)
     for dy in range(1, n_y):
         rec_products(dy)
-    attend_chunk(2)
-    forward_x(1)
-    hand_over(0, COLS, product(0, 0, rb, wor))
+    attend_chunk(1)
+    forward_x(0)
+    for c in range(SPLIT):
+        hand_over(0, COLS + c, product(0, c, rb, wor))
     rec_products(0)
     join_squares(0, channels * n_tp)
-    attend_chunk(1)
-    forward_x(0)
     attend_chunk(0)
 
     att_sq = jnp.zeros((rows, 1), F32)
@@ -635,10 +675,12 @@
         at = slice(h * VDIM, (h + 1) * VDIM)
         ab[:, at] = (att * again[:, at]).astype(BF16)
     share_squares(1, att_sq)
-    for dy in range(1, n_y):
-        hand_over(dy, 0, product(dy, 0, ab, woa))
-    for dy in range(1, n_y):
-        send_pair(dy, 0)
+    for c in range(SPLIT):
+        for dy in range(1, n_y):
+            hand_over(dy, c, product(dy, c, ab, woa))
+    for c in range(SPLIT):
+        for dy in range(1, n_y):
+            send_pair(dy, c)
     join_squares(1, heads * VDIM * n_tp)
 
     for dy in range(1, n_y):
@@ -647,21 +689,22 @@
             def _():
                 produce(dy, c)
 
-            @pl.when(c > 1)
+            @pl.when(c > SPLIT)
             def _():
                 send_pair(dy, c - 1)
 
             return 0
 
-        lax.fori_loop(1, COLS + 1, away, 0)
-
-    hand_over(0, 0, product(0, 0, ab, woa))
+        lax.fori_loop(SPLIT, COLS + 1, away, 0)
+
+    for c in range(SPLIT):
+        hand_over(0, c, product(0, c, ab, woa))
 
     def home(c, _):
         produce(0, c)
         return 0
 
-    lax.fori_loop(1, COLS, home, 0)
+    lax.fori_loop(SPLIT, COLS, home, 0)
 
     def gone(part, sem):
         remote(part, part, sem, own_sem.at[1], tp=partner).wait_send()
@@ -696,12 +739,12 @@
         return value
 
     @jax.named_scope("gather")
-    def first_columns():
+    def first_columns(c, total):
         count = cb // LANES
-        value = summed(COLS) * wide(inv[0, my_rows, :], count)
-        value = value + summed(0) * wide(inv[1, my_rows, :], count)
-        mixed[0] = value
-        return jnp.sum(value * value, axis=1, keepdims=True)
+        value = summed(COLS + c) * wide(inv[0, my_rows, :], count)
+        value = value + summed(c) * wide(inv[1, my_rows, :], count)
+        mixed[c] = value
+        return total + jnp.sum(value * value, axis=1, keepdims=True)
 
     @jax.named_scope("gather")
     def gather(c, total):
@@ -709,7 +752,8 @@
         mixed[c] = value
         return total + jnp.sum(value * value, axis=1, keepdims=True)
 
-    total = lax.fori_loop(1, COLS, gather, first_columns())
+    total = lax.fori_loop(0, SPLIT, first_columns, jnp.zeros((rd, 1), F32))
+    total = lax.fori_loop(SPLIT, COLS, gather, total)
 
     def out_copy(at):
         return pltpu.make_async_copy(done.at[:, at], out_ref.at[:, at], out_sem)
@@ -793,15 +837,15 @@
         vm((n_sp, 8, channels), F32), vm((2, 8, rows), F32), vm((2, n_tp, 8, rows), F32),
         vm((2, rows, LANES), F32),
         vm((n_y, COLS, 2 * rd, cb), F32), vm((2 * rd, cb), F32),
-        vm((n_y, COLS + 1, rd, cb), F32), vm((n_y, COLS + 1, rd, cb), BF16),
-        vm((n_y, COLS + 1, rd, cb), BF16), vm((n_y, COLS + 1, rd, cb), BF16),
-        vm((n_y, COLS + 1, rd, cb), BF16), vm((COLS, rd, cb), F32), vm((rd, width), BF16),
-        dma,
+        vm((n_y, COLS + SPLIT, rd, cb), F32), vm((n_y, COLS + SPLIT, rd, cb), BF16),
+        vm((n_y, COLS + SPLIT, rd, cb), BF16), vm((n_y, COLS + SPLIT, rd, cb), BF16),
+        vm((n_y, COLS + SPLIT, rd, cb), BF16), vm((COLS, rd, cb), F32), vm((rd, width), BF16),
+        dma, pltpu.SemaphoreType.REGULAR((max(1, (n_sp - 1) // 4 + 1),)),
         dma((16,)), dma((2, n_tp)), dma((2,)), dma, dma((n_y - 1, CHUNKS)),
         dma, dma((n_y - 1, CHUNKS)),
         dma, dma, dma, dma((n_sp // 2, CHUNKS)), dma((CHUNKS,)), dma((CHUNKS,)),
         dma((2,)), dma, dma, dma, dma((2,)),
-        dma, dma((n_y, COLS + 1)), dma, dma((n_y - 1, COLS + 1)),
+        dma, dma((n_y, COLS + SPLIT)), dma, dma((n_y - 1, COLS + SPLIT)),
     ]
     return pl.pallas_call(
         functools.partial(fused_kernel, n_sp, n_tp, heads),

time: 53.6 us -> 51.7 us (0.965)
  Pallas kernels: 51.6 us -> 49.6 us
    pallas_call x1, Pallas kernels: 51.6 us -> 49.6 us  [shards(): pl.pallas_call(functools.partial(fused_kernel, n_sp, n_tp, heads), out_sh...]
where the time goes in v4:
time: 51.7 us; the launch traced here: 51.5 us
  Pallas kernels  49.6 us (96%)
  local copies, waits for them, and re-layouts  1.87 us (4%)
    pallas_call x1, Pallas kernels, shards(): pl.pallas_call(functools.partial(fused_kernel, n_sp, n_tp, heads), out_sh...  49.6 us
    unnamed x1, local copies, waits for them, and re-layouts  1.87 us

profile of v4, /device:TPU:24, one launch (start us, length us, event | category | flops | bytes accessed | tf_op | source)
XLA Modules:
  0.0 51.5 jit_solution(14104382311519036127)
XLA Ops:
  0.0 49.6 %layer.1 = bf16[64,4096]{1,0:T(8,128)(2,1)} custom-call(bf16[256,1024]{1,0:T(8,128)(2,1)} %tokens.1, f32[4,1,1024]{2,1,0:T(1,128)} %bitcast.9, f32[1,256]{1,0:T(1,128)} %bitcast.12, bf16[4096,256]{1,0:T(8,128)(2,1)} %w_rec.1, bf16[4096,256]{1,0:T(8,128)(2,1)} %w_gate.1, f32[4,256]{1,0:T(4,128)} %taps_in.1, bf16[2,128,128]{2,1,0:T(8,128)(2,1)} %rmap_in.1, ...), custom_call_target="tpu_custom_call" | custom-call | tf_op jit(solution)/shard_map/layer/pallas_call | solution.py:850
  49.6 1.9 %copy.23 = bf16[64,4096]{1,0:T(8,128)(2,1)} copy(bf16[64,4096]{1,0:T(8,128)(2,1)} %layer.1) | data formatting | bytes 1048576

commit v5 on v4

--- a/solution.py
+++ b/solution.py
@@ -492,7 +492,7 @@
     pl.semaphore_wait(known.at[rounds - 1], near_count)
     lax.fori_loop(1, n_sp - me, carry_start, 0)
 
-    root = 1.0 / math.sqrt(NOPE + ROPE)
+    power = 1.0 / (math.sqrt(NOPE + ROPE) * math.log(2.0))
 
     @jax.named_scope("attend")
     def attend(keys_latent, keys_rope, limit):
@@ -501,19 +501,20 @@
             at = h * (NOPE + VDIM)
             keys = jnp.concatenate([expanded[:, at : at + NOPE], keys_rope], axis=1)
             values = expanded[:, at + NOPE : at + NOPE + VDIM]
-            scores = dot_t(qcat[h], keys) * root
-            k_at = lax.broadcasted_iota(jnp.int32, scores.shape, 1)
+            scores = dot_t(qcat[h], keys)
             if limit is None:
-                limit_at = lax.broadcasted_iota(jnp.int32, scores.shape, 0) + 1
+                q_at = lax.broadcasted_iota(jnp.int32, scores.shape, 0)
+                k_at = lax.broadcasted_iota(jnp.int32, scores.shape, 1)
+                scores = tiles(jnp.where(k_at <= q_at, scores, -jnp.inf))
             else:
-                limit_at = limit
-            scores = tiles(jnp.where(k_at < limit_at, scores, -jnp.inf))
+                k_at = lax.broadcasted_iota(jnp.int32, (1, scores.shape[1]), 1)
+                scores = tiles(scores + jnp.where(k_at < limit, 0.0, -jnp.inf))
             top = jnp.max(functools.reduce(jnp.maximum, scores), axis=1, keepdims=True)
             if limit is not None:
                 old = m_ref[h]
                 top = jnp.maximum(old, top)
-                shrink = jnp.exp(old - top)
-            weights = [jnp.exp(x - top) for x in scores]
+                shrink = jnp.exp2((old - top) * power)
+            weights = [jnp.exp2((x - top) * power) for x in scores]
             total = functools.reduce(jnp.add, weights)
             found = dot(jnp.concatenate([x.astype(BF16) for x in weights], axis=1), values)
             if limit is not None:
@@ -523,21 +524,26 @@
             l_ref[h] = total
             o_ref[h] = found
 
-    def attend_chunk(r):
-        def ready(k):
-            part = kv.at[0:k, 0:hc]
-            remote(part, part, kvd_tx, kvd_rx.at[r], tp=partner).wait_recv()
-
-        with jax.named_scope("kvwait"):
+    @jax.named_scope("kvwait")
+    def keys_ready(*chunks):
+        for r in chunks:
+            def ready(k):
+                part = kv.at[0:k, 0:hc]
+                remote(part, part, kvd_tx, kvd_rx.at[r], tp=partner).wait_recv()
+
             settle(me, n_sp - 1, ready)
+
+    def attend_chunks(*chunks):
+        span = len(chunks) * rc
+        at = pl.ds(min(chunks) * rc, span)
 
         def several(first, blocks):
             these = pl.ds(first, blocks)
-            count = blocks * rc
+            count = blocks * span
             attend(
-                kv[these, chunk(r), :latent].reshape(count, latent),
-                kv[these, chunk(r), latent:].reshape(count, LANES),
-                (me - first) * rc,
+                kv[these, at, :latent].reshape(count, latent),
+                kv[these, at, latent:].reshape(count, LANES),
+                (me - first) * span,
             )
 
         @pl.when((me > 0) & (me <= BATCH // 2))
@@ -644,7 +650,6 @@
     forward_x(3)
     attend(kv[me, :, :latent], kv[me, :, latent:], None)
     forward_z(0, 1, 2)
-    attend_chunk(3)
     forward_z(0, 2, 3)
     forward_z(1, 3, levels)
     forward_x(2)
@@ -653,31 +658,42 @@
         for c in range(SPLIT):
             hand_over(dy, COLS + c, product(dy, c, rb, wor))
     forward_z(0, 3, levels)
-    attend_chunk(2)
+    for dy in range(1, n_y):
+        rec_products(dy)
+    for c in range(SPLIT):
+        hand_over(0, COLS + c, product(0, c, rb, wor))
+    rec_products(0)
+    keys_ready(3, 2)
     for dy in range(1, n_y):
         for c in range(SPLIT):
             send_pair(dy, COLS + c)
     forward_x(1)
+    attend_chunks(3, 2)
+    forward_x(0)
+    keys_ready(1)
+    attend_chunks(1)
+    join_squares(0, channels * n_tp)
+    keys_ready(0)
+    attend_chunks(0)
+
+    def finish_attention(at):
+        squares = []
+        for h in range(heads):
+            att = o_ref[h, at, :] / jnp.sum(l_ref[h, at, :], axis=1, keepdims=True)
+            squares.append(att * att)
+            these = slice(h * VDIM, (h + 1) * VDIM)
+            ab[at, these] = (att * again[:, these]).astype(BF16)
+        sq[at, :] = functools.reduce(jnp.add, squares)
+
     for dy in range(1, n_y):
-        rec_products(dy)
-    attend_chunk(1)
-    forward_x(0)
-    for c in range(SPLIT):
-        hand_over(0, COLS + c, product(0, c, rb, wor))
-    rec_products(0)
-    join_squares(0, channels * n_tp)
-    attend_chunk(0)
-
-    att_sq = jnp.zeros((rows, 1), F32)
-    for h in range(heads):
-        att = o_ref[h] / jnp.sum(l_ref[h], axis=1, keepdims=True)
-        att_sq = att_sq + jnp.sum(att * att, axis=1, keepdims=True)
-        at = slice(h * VDIM, (h + 1) * VDIM)
-        ab[:, at] = (att * again[:, at]).astype(BF16)
-    share_squares(1, att_sq)
+        finish_attention(block(dy))
+        hand_over(dy, 0, product(dy, 0, ab, woa))
+    finish_attention(block(0))
+    share_squares(1, jnp.sum(sq[...], axis=1, keepdims=True))
     for c in range(SPLIT):
         for dy in range(1, n_y):
-            hand_over(dy, c, product(dy, c, ab, woa))
+            if c > 0:
+                hand_over(dy, c, product(dy, c, ab, woa))
     for c in range(SPLIT):
         for dy in range(1, n_y):
             send_pair(dy, c)

time: 51.7 us -> 50.9 us (0.985)
  Pallas kernels: 49.6 us -> 48.7 us
    pallas_call x1, Pallas kernels: 49.6 us -> 48.7 us  [shards(): pl.pallas_call(functools.partial(fused_kernel, n_sp, n_tp, heads), out_sh...]
where the time goes in v5:
time: 50.9 us; the launch traced here: 50.6 us
  Pallas kernels  48.7 us (96%)
  local copies, waits for them, and re-layouts  1.87 us (4%)
    pallas_call x1, Pallas kernels, shards(): pl.pallas_call(functools.partial(fused_kernel, n_sp, n_tp, heads), out_sh...  48.7 us
    unnamed x1, local copies, waits for them, and re-layouts  1.87 us

profile of v5, /device:TPU:24, one launch (start us, length us, event | category | flops | bytes accessed | tf_op | source)
XLA Modules:
  0.0 50.6 jit_solution(5701059479124156784)
XLA Ops:
  0.0 48.7 %layer.1 = bf16[64,4096]{1,0:T(8,128)(2,1)} custom-call(bf16[256,1024]{1,0:T(8,128)(2,1)} %tokens.1, f32[4,1,1024]{2,1,0:T(1,128)} %bitcast.9, f32[1,256]{1,0:T(1,128)} %bitcast.12, bf16[4096,256]{1,0:T(8,128)(2,1)} %w_rec.1, bf16[4096,256]{1,0:T(8,128)(2,1)} %w_gate.1, f32[4,256]{1,0:T(4,128)} %taps_in.1, bf16[2,128,128]{2,1,0:T(8,128)(2,1)} %rmap_in.1, ...), custom_call_target="tpu_custom_call" | custom-call | tf_op jit(solution)/shard_map/layer/pallas_call | solution.py:866
  48.7 1.9 %copy.23 = bf16[64,4096]{1,0:T(8,128)(2,1)} copy(bf16[64,4096]{1,0:T(8,128)(2,1)} %layer.1) | data formatting | bytes 1048576

commit v6 on v5

--- a/solution.py
+++ b/solution.py
@@ -670,11 +670,9 @@
     forward_x(1)
     attend_chunks(3, 2)
     forward_x(0)
-    keys_ready(1)
-    attend_chunks(1)
     join_squares(0, channels * n_tp)
-    keys_ready(0)
-    attend_chunks(0)
+    keys_ready(1, 0)
+    attend_chunks(1, 0)
 
     def finish_attention(at):
         squares = []

time: 50.9 us -> 50.4 us (level)
  no operation moved by 1% of the time
where the time goes in v6:
time: 50.4 us; the launch traced here: 50.3 us
  Pallas kernels  48.4 us (96%)
  local copies, waits for them, and re-layouts  1.87 us (4%)
    pallas_call x1, Pallas kernels, shards(): pl.pallas_call(functools.partial(fused_kernel, n_sp, n_tp, heads), out_sh...  48.4 us
    unnamed x1, local copies, waits for them, and re-layouts  1.87 us

profile of v6, /device:TPU:24, one launch (start us, length us, event | category | flops | bytes accessed | tf_op | source)
XLA Modules:
  0.0 50.3 jit_solution(14377452261782260738)
XLA Ops:
  0.0 48.4 %layer.1 = bf16[64,4096]{1,0:T(8,128)(2,1)} custom-call(bf16[256,1024]{1,0:T(8,128)(2,1)} %tokens.1, f32[4,1,1024]{2,1,0:T(1,128)} %bitcast.9, f32[1,256]{1,0:T(1,128)} %bitcast.12, bf16[4096,256]{1,0:T(8,128)(2,1)} %w_rec.1, bf16[4096,256]{1,0:T(8,128)(2,1)} %w_gate.1, f32[4,256]{1,0:T(4,128)} %taps_in.1, bf16[2,128,128]{2,1,0:T(8,128)(2,1)} %rmap_in.1, ...), custom_call_target="tpu_custom_call" | custom-call | tf_op jit(solution)/shard_map/layer/pallas_call | solution.py:864
  48.4 1.9 %copy.23 = bf16[64,4096]{1,0:T(8,128)(2,1)} copy(bf16[64,4096]{1,0:T(8,128)(2,1)} %layer.1) | data formatting | bytes 1048576
